TPU v7x, 32 devices: a whole 2x2x4 slice. The times are simulated.
32 devices in a mesh: grp: 2 (over y), sp: 4 (over z), tp: 4 (over x, core).
Axes of the slice: x: 2, y: 2, z: 4, core: 2. Of those that a mesh axis runs over, the one named last changes fastest.
Arguments:
- tokens: bfloat16 [2048, 4096], P(('grp', 'sp')), parts along dimension 0, may hold values from -6 to 6
- norm_gain: bfloat16 [2, 4096], replicated, may hold values from 0.099609375 to 1.8984375
- w_query: bfloat16 [2, 4096, 2048], P(None, 'sp', 'tp'), may hold values from -0.09375 to 0.09375
- w_key: bfloat16 [2, 4096, 2048], P(None, 'sp', 'tp'), may hold values from -0.09375 to 0.09375
- w_value: bfloat16 [2, 4096, 2048], P(None, 'sp', 'tp'), may hold values from -0.09375 to 0.09375
- w_out: bfloat16 [2, 2048, 4096], P(None, 'tp', 'sp'), may hold values from -0.125 to 0.125
- offset_bias: float32 [2, 16, 15, 31], P(None, 'tp'), may hold values from -4 to 300
Outputs:
- mixed: bfloat16 [2048, 4096], P(('grp', 'sp')), parts along dimension 0
There are 2 independent parts, one for each index of `grp`. A program takes and returns all parts, laid end to end along the dimension named above; an argument that names none is the same for every part. Nothing has to cross between parts.
All inputs are finite; a program needn't handle non-finite values.
Results may differ from a plain program's by a relative error of at most 0.013.
Values may be sent and summed in bfloat16 or wider, within the bound.
A program may use at most 128 MiB of HBM per device.

v0:
```python
import functools

import jax
import jax.numpy as jnp
from jax import lax
from jax.experimental import pallas as pl
from jax.experimental.pallas import tpu as pltpu
from jax.sharding import PartitionSpec as P

HD = 128
GRID_W = 64
KR = 8
KC = 16
LAYERS = 2


norm_eps = 1e-06


def with_halo(block, sides, width):
    for axis, dim in sides:
        count = lax.axis_size(axis)
        forward = [(i, i + 1) for i in range(count - 1)]
        backward = [(target, source) for source, target in forward]
        low = lax.ppermute(
            lax.slice_in_dim(block, block.shape[dim] - width, None, axis=dim), axis, forward
        )
        high = lax.ppermute(lax.slice_in_dim(block, 0, width, axis=dim), axis, backward)
        block = jnp.concatenate([low, block, high], axis=dim)
    return block


def rms_rows(values, gain):
    wide = values.astype(jnp.float32)
    scaled = wide * lax.rsqrt(jnp.mean(wide * wide, axis=-1, keepdims=True) + norm_eps)
    return (scaled * gain.astype(jnp.float32)).astype(jnp.bfloat16)


def general(tokens, norm_gain, w_query, w_key, w_value, w_out, offset_bias):
    sp_count = lax.axis_size("sp")
    sp_index = lax.axis_index("sp")
    tok_rows = tokens.shape[0]
    local_rows = tok_rows // GRID_W
    grid_rows = local_rows * sp_count
    heads_here = offset_bias.shape[1]
    head_width = heads_here * HD
    reach = KR // 2
    scale = HD ** (-0.5)
    columns = jnp.arange(GRID_W, dtype=jnp.int32)
    col_first = jnp.clip(columns - KC // 2, 0, GRID_W - KC)
    col_inside = (columns[None, :] >= col_first[:, None]) & (
        columns[None, :] < col_first[:, None] + KC
    )
    col_offset = jnp.clip(columns[None, :] - columns[:, None], 1 - KC, KC - 1) + KC - 1
    col_onehot = (
        jnp.arange(2 * KC - 1, dtype=jnp.int32)[:, None, None] == col_offset[None, :, :]
    ).astype(jnp.float32)
    first_row = sp_index * local_rows
    own_rows = first_row + jnp.arange(local_rows, dtype=jnp.int32)
    row_first = jnp.clip(own_rows - reach, 0, grid_rows - KR)
    band_start = row_first - first_row + reach
    row_offset = (
        row_first[:, None] + jnp.arange(KR, dtype=jnp.int32)[None, :] - own_rows[:, None] + KR - 1
    )
    row_onehot = (
        row_offset[:, :, None] == jnp.arange(2 * KR - 1, dtype=jnp.int32)[None, None, :]
    ).astype(jnp.float32)
    qkv_weight = jnp.concatenate([w_query, w_key, w_value], axis=2)
    residual = lax.all_to_all(tokens, "sp", split_axis=1, concat_axis=0, tiled=True)
    width = residual.shape[1]
    features = width * sp_count
    for layer_index in range(LAYERS):
        wide = residual.astype(jnp.float32)
        squares = lax.psum_scatter(
            jnp.sum(wide * wide, axis=-1, keepdims=True), "sp", scatter_dimension=0, tiled=True
        )
        inverse = lax.rsqrt(squares / features + norm_eps)
        gain = lax.dynamic_slice_in_dim(norm_gain[layer_index], sp_index * width, width, 0)
        gained = (wide * gain.astype(jnp.float32)).astype(jnp.bfloat16)
        partial = jnp.dot(gained, qkv_weight[layer_index], preferred_element_type=jnp.float32)
        mine = lax.psum_scatter(
            partial.astype(jnp.bfloat16), "sp", scatter_dimension=0, tiled=True
        )
        mine = (mine.astype(jnp.float32) * inverse).astype(jnp.bfloat16)
        queries = mine[:, :head_width].reshape(local_rows, GRID_W, heads_here, HD)
        key_values = mine[:, head_width:].reshape(local_rows, GRID_W, 2 * head_width)
        padded = with_halo(key_values, (("sp", 0),), reach)
        bands = jax.vmap(lambda band_begin: lax.dynamic_slice_in_dim(padded, band_begin, KR, 0))(
            band_start
        )
        band_keys = bands[..., :head_width].reshape(local_rows, KR, GRID_W, heads_here, HD)
        band_values = bands[..., head_width:].reshape(local_rows, KR, GRID_W, heads_here, HD)
        col_bias = jnp.einsum(
            "hro,oqk->hrqk", offset_bias[layer_index], col_onehot, precision=lax.Precision.HIGHEST
        )
        full_bias = jnp.einsum(
            "ijr,hrqk->hiqjk", row_onehot, col_bias, precision=lax.Precision.HIGHEST
        )
        scores = jnp.einsum(
            "iqhd,ijkhd->hiqjk", queries, band_keys, preferred_element_type=jnp.float32
        )
        scores = scores * scale + full_bias
        scores = jnp.where(col_inside[None, None, :, None, :], scores, -jnp.inf)
        flattened = scores.reshape(heads_here, local_rows, GRID_W, KR * GRID_W)
        weights = jax.nn.softmax(flattened, axis=-1).astype(jnp.bfloat16)
        weights = weights.reshape(heads_here, local_rows, GRID_W, KR, GRID_W)
        attended = jnp.einsum(
            "hiqjk,ijkhd->iqhd", weights, band_values, preferred_element_type=jnp.float32
        )
        attended = attended.astype(jnp.bfloat16).reshape(tok_rows, head_width)
        every = lax.all_gather(attended, "sp", axis=0, tiled=True)
        share = jnp.dot(every, w_out[layer_index], preferred_element_type=jnp.float32)
        branch = lax.psum(share.astype(jnp.bfloat16), "tp").astype(jnp.float32)
        residual = (residual.astype(jnp.float32) + branch).astype(jnp.bfloat16)
    return lax.all_to_all(residual, "sp", split_axis=0, concat_axis=1, tiled=True)


MESH = pl.DeviceIdType.MESH
VMEM_MOST = 60 * 2**20
CHUNK = 128
PIECE = 64
LAG = 2


def greet(peers):
    barrier = pltpu.get_barrier_semaphore()
    for axis, index in peers:
        pl.semaphore_signal(barrier, inc=1, device_id={axis: index}, device_id_type=MESH)
    pl.semaphore_wait(barrier, len(peers))


def remote(src, dst, send, recv, axis, index):
    return pltpu.make_async_remote_copy(
        src_ref=src, dst_ref=dst, send_sem=send, recv_sem=recv,
        device_id={axis: index}, device_id_type=MESH,
    )


def span(start, size):
    return pl.ds(pl.multiple_of(start, size), size)


def spread_kernel(n, tok_ref, x_ref, send, recv, far_send, far_recv):
    me, t = lax.axis_index("sp"), lax.axis_index("tp")
    half = lax.rem(t, 2)
    partner = t + 1 - 2 * half
    rows, width = tok_ref.shape[0], tok_ref.shape[1] // n
    part = width // 2
    greet([("sp", lax.rem(me + k, n)) for k in range(1, n)] + [("tp", partner)])
    lanes = span(half * part, part)
    sent = []
    for k in range(1, n):
        to = lax.rem(me + k, n)
        copy = remote(
            tok_ref.at[:, span(to * width + half * part, part)],
            x_ref.at[span(me * rows, rows), lanes],
            send.at[k - 1], recv.at[k - 1], "sp", to,
        )
        copy.start()
        sent.append(copy)
    x_ref[span(me * rows, rows), :] = tok_ref[:, span(me * width, width)]
    passed = []
    for k in range(1, n):
        source = lax.rem(me + n - k, n)
        sent[k - 1].wait_recv()
        here = x_ref.at[span(source * rows, rows), lanes]
        copy = remote(here, here, far_send.at[k - 1], far_recv.at[k - 1], "tp", partner)
        copy.start()
        passed.append(copy)
    for k in range(n - 1):
        sent[k].wait_send()
        passed[k].wait()


def project_kernel(
    n, layer, features, x_ref, gain_ref, wq_ref, wk_ref, wv_ref, out_ref,
    gained, inbox, outbox, acc, sq_own, sq_in, inverse,
    send, recv, sq_send, sq_recv,
):
    me = lax.axis_index("sp")
    tokens, width = x_ref.shape
    cols = wq_ref.shape[1] // 2
    pieces = tokens // PIECE
    greet([("sp", lax.rem(me + k, n)) for k in range(1, n)])
    gain = gain_ref[pl.ds(layer, 1), span(me * width, width)].astype(jnp.float32)
    ones = jnp.ones((8, width), jnp.float32)

    @pl.loop(0, tokens // CHUNK)
    def _(i):
        rows = span(i * CHUNK, CHUNK)
        wide = x_ref[rows, :].astype(jnp.float32)
        gained[rows, :] = (wide * gain).astype(jnp.bfloat16)
        sq_own[:, rows] = lax.dot_general(
            ones, wide * wide, (((1,), (1,)), ((), ())),
            precision=lax.Precision.HIGHEST, preferred_element_type=jnp.float32,
        )

    ends = (n - 1, 0)
    for e, end in enumerate(ends):
        @pl.when(me != end)
        def _(e=e, end=end):
            remote(sq_own, sq_in.at[me], sq_send.at[e], sq_recv.at[me], "sp", end).start()

    at_end = (me == 0) | (me == n - 1)

    @pl.when(at_end)
    def _():
        for k in range(1, n):
            source = lax.rem(me + k, n)
            remote(sq_own, sq_in.at[source], sq_send.at[0], sq_recv.at[source], "sp", source).wait_recv()
        sq_in[me] = sq_own[...]

        @pl.loop(0, tokens // CHUNK)
        def _(i):
            rows = span(i * CHUNK, CHUNK)
            total = sq_in[0, :, rows]
            for k in range(1, n):
                total = total + sq_in[k, :, rows]
            scaled = lax.rsqrt(total / features + norm_eps)
            inverse[rows, :] = jnp.concatenate([scaled] * (CHUNK // 8), axis=0).T

    def flow(way, piece):
        place = me if way == 0 else n - 1 - me
        after = me + 1 if way == 0 else me - 1
        rows = span(piece * PIECE, PIECE)
        lo = (1 - way) * cols
        for j, w_ref in enumerate((wq_ref, wk_ref, wv_ref)):
            acc[:, j * cols:(j + 1) * cols] = jnp.dot(
                gained[rows, :], w_ref[:, lo:lo + cols], preferred_element_type=jnp.float32
            )

        def copy():
            return remote(
                outbox.at[way, rows, :], inbox.at[way, rows, :],
                send.at[way, piece], recv.at[way, piece], "sp", after,
            )

        @pl.when(place > 0)
        def _():
            copy().wait_recv()
            acc[...] += inbox[way, rows, :].astype(jnp.float32)

        @pl.when(place < n - 1)
        def _():
            outbox[way, rows, :] = acc[...].astype(jnp.bfloat16)
            copy().start()

        @pl.when(place == n - 1)
        def _():
            out_ref[rows, :] = (acc[...] * inverse[rows, :1]).astype(jnp.bfloat16)

    @pl.loop(0, pieces + (n - 1) * LAG)
    def _(step):
        for way in range(2):
            place = me if way == 0 else n - 1 - me
            piece = step - place * LAG

            @pl.when((piece >= 0) & (piece < pieces))
            def _(way=way, piece=piece):
                flow(way, piece)

    @pl.when(jnp.logical_not(at_end))
    def _():
        out_ref[...] = jnp.zeros_like(out_ref)

    for e, end in enumerate(ends):
        @pl.when(me != end)
        def _(e=e, end=end):
            remote(sq_own, sq_in.at[me], sq_send.at[e], sq_recv.at[me], "sp", end).wait_send()

            @pl.loop(0, pieces)
            def _(i):
                rows = span(i * PIECE, PIECE)
                remote(
                    outbox.at[e, rows, :], inbox.at[e, rows, :],
                    send.at[e, i], recv.at[e, i], "sp", end,
                ).wait_send()


def attend_kernel(heads, rows, scale, mine_ref, bias_ref, out_ref):
    cols = heads * HD
    for h in range(heads):
        for r in range(rows):
            first = min(max(r - KR // 2, 0), rows - KR)
            q = mine_ref[r * GRID_W:(r + 1) * GRID_W, h * HD:(h + 1) * HD]
            band = slice(first * GRID_W, (first + KR) * GRID_W)
            k = mine_ref[band, cols + h * HD:cols + (h + 1) * HD]
            v = mine_ref[band, 2 * cols + h * HD:2 * cols + (h + 1) * HD]
            scores = lax.dot_general(
                q, k, (((1,), (1,)), ((), ())), preferred_element_type=jnp.float32
            )
            scores = scores * scale + bias_ref[h, first - r + KR - 1]
            scores = jnp.exp(scores - jnp.max(scores, axis=-1, keepdims=True))
            weights = scores / jnp.sum(scores, axis=-1, keepdims=True)
            out = jnp.dot(weights.astype(jnp.bfloat16), v, preferred_element_type=jnp.float32)
            out_ref[r * GRID_W:(r + 1) * GRID_W, h * HD:(h + 1) * HD] = out.astype(jnp.bfloat16)


def combine_kernel(
    n, m, last, att_ref, x_ref, w_ref, out_ref,
    box, give, take, pair, cross_in, fresh,
    send, recv, give_s, give_r, cross_s, cross_r, fresh_s, fresh_r, far_s, far_r,
):
    me, t = lax.axis_index("sp"), lax.axis_index("tp")
    half = lax.rem(t, 2)
    partner = t + 1 - 2 * half
    cross = lax.rem(t + m // 2, m)
    tokens, width = x_ref.shape
    cols = att_ref.shape[1]
    part = width // 2
    chunks = tokens // CHUNK
    per = chunks // n
    lanes = span(half * part, part)
    other = span((1 - half) * part, part)
    greet(
        [("sp", lax.rem(me + k, n)) for k in range(1, n)] + [("tp", partner), ("tp", cross)]
    )

    def where(step):
        return span((lax.rem(step, n) * per + step // n) * CHUNK, CHUNK)

    def hop(way, step, source=None):
        rows = where(step)
        src = box.at[way, rows, :] if source is None else source.at[rows, :]
        after = me + 1 if way == 0 else me - 1
        return remote(src, box.at[way, rows, :], send.at[way, step], recv.at[way, step], "sp", after)

    for way, start in ((0, 0), (1, n - 1)):
        @pl.when(me == start)
        def _(way=way):
            @pl.loop(0, chunks)
            def _(i):
                hop(way, i, att_ref).start()
            box[way] = att_ref[...]

    def onward(way, step):
        place = me if way == 0 else n - 1 - me

        @pl.when(place > 0)
        def _():
            hop(way, step).wait_recv()

            @pl.when(place < n - 1)
            def _():
                hop(way, step).start()

    def forward(step):
        @pl.when(me < n // 2)
        def _():
            onward(0, step)
            onward(1, step)

        @pl.when(me >= n // 2)
        def _():
            onward(1, step)
            onward(0, step)

    def give_copy(step):
        rows = where(step)
        return remote(give.at[rows, :], take.at[rows, :], give_s.at[step], give_r.at[step], "tp", partner)

    def cross_copy(step):
        rows = where(step)
        return remote(
            pair.at[rows, :], cross_in.at[rows, :], cross_s.at[step], cross_r.at[step], "tp", cross
        )

    def multiply(step):
        rows = where(step)

        def share(at):
            return jnp.dot(
                box[0, rows, :], w_ref[:cols, at], preferred_element_type=jnp.float32
            ) + jnp.dot(box[1, rows, :], w_ref[cols:, at], preferred_element_type=jnp.float32)

        give[rows, :] = share(other).astype(jnp.bfloat16)
        give_copy(step).start()
        pair[rows, :] = share(lanes).astype(jnp.bfloat16)

    def meet(step):
        rows = where(step)
        give_copy(step).wait_recv()
        pair[rows, :] = (
            pair[rows, :].astype(jnp.float32) + take[rows, :].astype(jnp.float32)
        ).astype(jnp.bfloat16)
        cross_copy(step).start()

    def fresh_copy(step):
        rows = where(step)
        if not last:
            return remote(
                fresh.at[rows, :], out_ref.at[rows, lanes], fresh_s.at[step], fresh_r.at[step], "tp", partner
            )
        return remote(
            fresh.at[rows, :],
            out_ref.at[span(step // n * CHUNK, CHUNK), span(me * width + half * part, part)],
            fresh_s.at[step], fresh_r.at[me, step // n], "sp", lax.rem(step, n),
        )

    def finish(step):
        rows = where(step)
        cross_copy(step).wait_recv()
        branch = pair[rows, :].astype(jnp.float32) + cross_in[rows, :].astype(jnp.float32)
        new = (x_ref[rows, lanes].astype(jnp.float32) + branch).astype(jnp.bfloat16)
        if not last:
            fresh[rows, :] = new
            fresh_copy(step).start()
            out_ref[rows, lanes] = new
            return

        @pl.when(lax.rem(step, n) == me)
        def _():
            out_ref[span(step // n * CHUNK, CHUNK), span(me * width + half * part, part)] = new

        @pl.when(lax.rem(step, n) != me)
        def _():
            fresh[rows, :] = new
            fresh_copy(step).start()

    stages = ((forward, 0), (multiply, 1), (meet, 2), (finish, 4))

    @pl.loop(0, chunks + 4)
    def _(step):
        for stage, late in stages:
            at = step - late

            @pl.when((at >= 0) & (at < chunks))
            def _(stage=stage, at=at):
                stage(at)

    if last:
        def far_copy(source, q):
            here = out_ref.at[span(q * CHUNK, CHUNK), span(source * width + half * part, part)]
            return remote(here, here, far_s.at[source, q], far_r.at[source, q], "tp", partner)

        for q in range(per):
            for k in range(n):
                source = lax.rem(me + k, n)
                if k > 0:
                    here = out_ref.at[span(q * CHUNK, CHUNK), span(source * width + half * part, part)]
                    remote(
                        here, here, far_s.at[source, q], fresh_r.at[source, q], "sp", source
                    ).wait_recv()
                far_copy(source, q).start()
        for q in range(per):
            for k in range(n):
                source = lax.rem(me + k, n)
                there = out_ref.at[span(q * CHUNK, CHUNK), span(source * width + (1 - half) * part, part)]
                remote(there, there, far_s.at[source, q], far_r.at[source, q], "tp", partner).wait_recv()
                far_copy(source, q).wait_send()

    @pl.loop(0, chunks)
    def _(i):
        give_copy(i).wait_send()
        cross_copy(i).wait_send()
        if not last:
            rows = where(i)
            fresh_copy(i).wait_send()
            remote(
                fresh.at[rows, :], out_ref.at[rows, other], fresh_s.at[i], fresh_r.at[i], "tp", partner
            ).wait_recv()
        else:
            @pl.when(lax.rem(i, n) != me)
            def _():
                fresh_copy(i).wait_send()
        for way, end in ((0, n - 1), (1, 0)):
            @pl.when(me != end)
            def _(way=way):
                hop(way, i).wait_send()


def vmem():
    return pl.BlockSpec(memory_space=pltpu.VMEM)


def of_layer(array, layer):
    rest = array.shape[1:]
    return pl.BlockSpec((None, *rest), lambda i: (layer, *(0 for _ in rest)))


def params(identity):
    return pltpu.CompilerParams(
        collective_id=identity, has_side_effects=True, vmem_limit_bytes=VMEM_MOST
    )


def staged(tokens, norm_gain, w_query, w_key, w_value, w_out, offset_bias):
    n, m = lax.axis_size("sp"), lax.axis_size("tp")
    me = lax.axis_index("sp")
    own, features = tokens.shape
    width, total = features // n, own * n
    grid_rows = total // GRID_W
    heads = offset_bias.shape[1] // 2
    cols = heads * HD
    dma = pltpu.SemaphoreType.DMA
    bf16, f32 = jnp.bfloat16, jnp.float32

    columns = jnp.arange(GRID_W, dtype=jnp.int32)
    col_first = jnp.clip(columns - KC // 2, 0, GRID_W - KC)
    inside = (columns[None, :] >= col_first[:, None]) & (columns[None, :] < col_first[:, None] + KC)
    offset = jnp.clip(columns[None, :] - columns[:, None], 1 - KC, KC - 1) + KC - 1
    onehot = (
        jnp.arange(2 * KC - 1, dtype=jnp.int32)[:, None, None] == offset[None, :, :]
    ).astype(f32)
    table = lax.dynamic_slice_in_dim(offset_bias, jnp.where(me == n - 1, heads, 0), heads, 1)
    table = jnp.stack([table[:, :, a:a + KR] for a in range(KR)], axis=2)
    bias = jnp.einsum("lhajo,oqk->lhaqjk", table, onehot, precision=lax.Precision.HIGHEST)
    bias = jnp.where(inside[:, None, :], bias, -jnp.inf)
    bias = bias.reshape(LAYERS, heads, KR, GRID_W, KR * GRID_W)

    x = pl.pallas_call(
        functools.partial(spread_kernel, n),
        out_shape=jax.ShapeDtypeStruct((total, width), bf16),
        in_specs=[vmem()],
        grid=(1,),
        out_specs=vmem(),
        scratch_shapes=[dma((n - 1,))] * 4,
        compiler_params=params(1),
        name="spread",
    )(tokens)
    pieces, chunks = total // PIECE, total // CHUNK
    for layer in range(LAYERS):
        last = layer == LAYERS - 1
        mine = pl.pallas_call(
            functools.partial(project_kernel, n, layer, features),
            out_shape=jax.ShapeDtypeStruct((total, 3 * cols), bf16),
            in_specs=[vmem(), vmem()] + [of_layer(w, layer) for w in (w_query, w_key, w_value)],
            grid=(1,),
            out_specs=vmem(),
            scratch_shapes=[
                pltpu.VMEM((total, width), bf16),
                pltpu.VMEM((2, total, 3 * cols), bf16),
                pltpu.VMEM((2, total, 3 * cols), bf16),
                pltpu.VMEM((PIECE, 3 * cols), f32),
                pltpu.VMEM((8, total), f32),
                pltpu.VMEM((n, 8, total), f32),
                pltpu.VMEM((total, CHUNK), f32),
                dma((2, pieces)), dma((2, pieces)), dma((2,)), dma((n,)),
            ],
            compiler_params=params(2 + 2 * layer),
            name="project",
        )(x, norm_gain, w_query, w_key, w_value)
        attended = pl.pallas_call(
            functools.partial(attend_kernel, heads, grid_rows, HD ** (-0.5)),
            out_shape=jax.ShapeDtypeStruct((total, cols), bf16),
            in_specs=[vmem(), of_layer(bias, layer)],
            grid=(1,),
            out_specs=vmem(),
            compiler_params=pltpu.CompilerParams(vmem_limit_bytes=VMEM_MOST),
            name="attend",
        )(mine, bias)
        x = pl.pallas_call(
            functools.partial(combine_kernel, n, m, last),
            out_shape=jax.ShapeDtypeStruct((own, features) if last else (total, width), bf16),
            in_specs=[vmem(), vmem(), of_layer(w_out, layer)],
            grid=(1,),
            out_specs=vmem(),
            scratch_shapes=[
                pltpu.VMEM((2, total, cols), bf16),
                *[pltpu.VMEM((total, width // 2), bf16)] * 5,
                dma((2, chunks)), dma((2, chunks)),
                *[dma((chunks,))] * 4,
                dma((chunks,)),
                dma((n, chunks // n)) if last else dma((chunks,)),
                dma((n, chunks // n)), dma((n, chunks // n)),
            ],
            compiler_params=params(3 + 2 * layer),
            name="combine",
        )(attended, x, w_out)
    return x


def on_device(tokens, norm_gain, w_query, w_key, w_value, w_out, offset_bias):
    n, m = lax.axis_size("sp"), lax.axis_size("tp")
    own, features = tokens.shape
    total, width = own * n, features // n
    fits = total * (6 * width + 8 * w_query.shape[2]) * 2 < VMEM_MOST // 2
    even = offset_bias.shape[1] % 2 == 0 and m == 4 and n > 1
    if fits and even and own % CHUNK == 0 and width % 256 == 0:
        return staged(tokens, norm_gain, w_query, w_key, w_value, w_out, offset_bias)
    return general(tokens, norm_gain, w_query, w_key, w_value, w_out, offset_bias)


def solution(mesh):
    return jax.shard_map(
        on_device,
        mesh=mesh,
        in_specs=(
            P(("grp", "sp"), None),
            P(),
            P(None, "sp", "tp"),
            P(None, "sp", "tp"),
            P(None, "sp", "tp"),
            P(None, "tp", "sp"),
            P(None, "tp", None, None),
        ),
        out_specs=P(("grp", "sp"), None),
        check_vma=False,
    )
```

profile of v0, /device:TPU:29, one launch (start us, length us, event | category | flops | bytes accessed | tf_op | source)
XLA Modules:
  0.0 331.4 jit_solution(10404792191586805175)
XLA Ops:
  0.0 1.1 constant_dynamic-slice_fusion.7
  1.2 0.1 fusion.4
  1.4 5.6 %select_bitcast_fusion = f32[2,2,8,64,8,64]{5,4,2,1,0,3:T(8,128)} fusion(pred[64,64]{1,0:T(8,128)(4,1)S(1)} %fusion.4, s32[64,64]{1,0:T(8,128)S(1)} %clamp_add_fusion, f32[2,2,8,8,31]{4,3,2,1,0:T(8,128)S(1)} %constant_dynamic-update-slice_fusion), kind=kOutput, calls=%fused_computation | convolution fusion | flops 391245824 | bytes 4246528 | tf_op jit(solution)/shard_map/lhajo,oqk->lhaqjk/dot_general | solution.py:507
  7.0 7.5 %reshape.29 = f32[2,2,8,64,512]{4,2,1,0,3:T(8,128)} reshape(f32[2,2,8,64,8,64]{5,4,2,1,0,3:T(8,128)} %select_bitcast_fusion) | data formatting | bytes 8388608 | tf_op jit(solution)/shard_map/reshape | solution.py:509
  14.5 6.5 %copy.18.bias_ref = f32[2,2,8,64,512]{4,3,2,1,0:T(8,128)} copy(f32[2,2,8,64,512]{4,2,1,0,3:T(8,128)} %reshape.29) | data formatting | bytes 8388608 | tf_op jit(solution)/shard_map/reshape | solution.py:509
  21.0 30.9 %spread.1.x_ref = bf16[1024,1024]{1,0:T(8,128)(2,1)} custom-call(bf16[256,4096]{1,0:T(8,128)(2,1)} %tok_ref.1), custom_call_target="tpu_custom_call" | custom-call | tf_op jit(solution)/shard_map/spread/pallas_call | solution.py:511
  51.9 58.4 %project.2.mine_ref = bf16[1024,768]{1,0:T(8,128)(2,1)} custom-call(bf16[1024,1024]{1,0:T(8,128)(2,1)} %spread.1.x_ref, bf16[2,4096]{1,0:T(2,128)(2,1)} %gain_ref.3, bf16[2,1024,512]{2,1,0:T(8,128)(2,1)} %wq_ref.3, bf16[2,1024,512]{2,1,0:T(8,128)(2,1)} %wk_ref.3, bf16[2,1024,512]{2,1,0:T(8,128)(2,1)} %wv_ref.3), custom_call_target="tpu_custom_call" | custom-call | tf_op jit(solution)/shard_map/project/pallas_call | solution.py:524
  110.3 13.7 %attend.2.att_ref = bf16[1024,256]{1,0:T(8,128)(2,1)} custom-call(bf16[1024,768]{1,0:T(8,128)(2,1)} %project.2.mine_ref, f32[2,2,8,64,512]{4,3,2,1,0:T(8,128)} %copy.18.bias_ref), custom_call_target="tpu_custom_call" | custom-call | tf_op jit(solution)/shard_map/attend/pallas_call | solution.py:543
  124.1 57.6 %combine.2.x_ref = bf16[1024,1024]{1,0:T(8,128)(2,1)} custom-call(bf16[1024,256]{1,0:T(8,128)(2,1)} %attend.2.att_ref, bf16[1024,1024]{1,0:T(8,128)(2,1)} %spread.1.x_ref, bf16[2,512,1024]{2,1,0:T(8,128)(2,1)} %w_ref.3), custom_call_target="tpu_custom_call" | custom-call | tf_op jit(solution)/shard_map/combine/pallas_call | solution.py:552
  181.7 56.8 %project.3.mine_ref = bf16[1024,768]{1,0:T(8,128)(2,1)} custom-call(bf16[1024,1024]{1,0:T(8,128)(2,1)} %combine.2.x_ref, bf16[2,4096]{1,0:T(2,128)(2,1)} %gain_ref.3, bf16[2,1024,512]{2,1,0:T(8,128)(2,1)} %wq_ref.3, bf16[2,1024,512]{2,1,0:T(8,128)(2,1)} %wk_ref.3, bf16[2,1024,512]{2,1,0:T(8,128)(2,1)} %wv_ref.3), custom_call_target="tpu_custom_call" | custom-call | tf_op jit(solution)/shard_map/project/pallas_call | solution.py:524
  238.5 13.7 %attend.3.att_ref = bf16[1024,256]{1,0:T(8,128)(2,1)} custom-call(bf16[1024,768]{1,0:T(8,128)(2,1)} %project.3.mine_ref, f32[2,2,8,64,512]{4,3,2,1,0:T(8,128)} %copy.18.bias_ref), custom_call_target="tpu_custom_call" | custom-call | tf_op jit(solution)/shard_map/attend/pallas_call | solution.py:543
  252.2 76.1 %combine.3 = bf16[256,4096]{1,0:T(8,128)(2,1)} custom-call(bf16[1024,256]{1,0:T(8,128)(2,1)} %attend.3.att_ref, bf16[1024,1024]{1,0:T(8,128)(2,1)} %combine.2.x_ref, bf16[2,512,1024]{2,1,0:T(8,128)(2,1)} %w_ref.3), custom_call_target="tpu_custom_call" | custom-call | tf_op jit(solution)/shard_map/combine/pallas_call | solution.py:552
  328.3 3.1 copy.60
  (10 shorter events, 0.0 us)
where the time goes:
time: 334 us; the launch traced here: 331 us
  Pallas kernels  307 us (92%)
  local copies, waits for them, and re-layouts  18.3 us (5%)
  matrix products  5.63 us (2%)
    pallas_call x2, Pallas kernels, staged(): pl.pallas_call(functools.partial(combine_kernel, n, m, last), out_shape=j...  134 us
    pallas_call x2, Pallas kernels, staged(): pl.pallas_call(functools.partial(project_kernel, n, layer, features), out...  115 us
    pallas_call x1, Pallas kernels, staged(): pl.pallas_call(functools.partial(spread_kernel, n), out_shape=jax.ShapeDt...  30.9 us
    pallas_call x2, Pallas kernels, staged(): pl.pallas_call(functools.partial(attend_kernel, heads, grid_rows, HD ** (...  27.5 us
    reshape x2, local copies, waits for them, and re-layouts, staged(): bias = bias.reshape(LAYERS, heads, KR, GRID_W, KR * GRID_W)  14 us

commit v1 on v0

v1 whole, which is shorter than its diff:
```python
import functools

import jax
import jax.numpy as jnp
from jax import lax
from jax.experimental import pallas as pl
from jax.experimental.pallas import tpu as pltpu
from jax.sharding import PartitionSpec as P

HD = 128
GRID_W = 64
KR = 8
KC = 16
LAYERS = 2


norm_eps = 1e-06


def with_halo(block, sides, width):
    for axis, dim in sides:
        count = lax.axis_size(axis)
        forward = [(i, i + 1) for i in range(count - 1)]
        backward = [(target, source) for source, target in forward]
        low = lax.ppermute(
            lax.slice_in_dim(block, block.shape[dim] - width, None, axis=dim), axis, forward
        )
        high = lax.ppermute(lax.slice_in_dim(block, 0, width, axis=dim), axis, backward)
        block = jnp.concatenate([low, block, high], axis=dim)
    return block


def rms_rows(values, gain):
    wide = values.astype(jnp.float32)
    scaled = wide * lax.rsqrt(jnp.mean(wide * wide, axis=-1, keepdims=True) + norm_eps)
    return (scaled * gain.astype(jnp.float32)).astype(jnp.bfloat16)


def general(tokens, norm_gain, w_query, w_key, w_value, w_out, offset_bias):
    sp_count = lax.axis_size("sp")
    sp_index = lax.axis_index("sp")
    tok_rows = tokens.shape[0]
    local_rows = tok_rows // GRID_W
    grid_rows = local_rows * sp_count
    heads_here = offset_bias.shape[1]
    head_width = heads_here * HD
    reach = KR // 2
    scale = HD ** (-0.5)
    columns = jnp.arange(GRID_W, dtype=jnp.int32)
    col_first = jnp.clip(columns - KC // 2, 0, GRID_W - KC)
    col_inside = (columns[None, :] >= col_first[:, None]) & (
        columns[None, :] < col_first[:, None] + KC
    )
    col_offset = jnp.clip(columns[None, :] - columns[:, None], 1 - KC, KC - 1) + KC - 1
    col_onehot = (
        jnp.arange(2 * KC - 1, dtype=jnp.int32)[:, None, None] == col_offset[None, :, :]
    ).astype(jnp.float32)
    first_row = sp_index * local_rows
    own_rows = first_row + jnp.arange(local_rows, dtype=jnp.int32)
    row_first = jnp.clip(own_rows - reach, 0, grid_rows - KR)
    band_start = row_first - first_row + reach
    row_offset = (
        row_first[:, None] + jnp.arange(KR, dtype=jnp.int32)[None, :] - own_rows[:, None] + KR - 1
    )
    row_onehot = (
        row_offset[:, :, None] == jnp.arange(2 * KR - 1, dtype=jnp.int32)[None, None, :]
    ).astype(jnp.float32)
    qkv_weight = jnp.concatenate([w_query, w_key, w_value], axis=2)
    residual = lax.all_to_all(tokens, "sp", split_axis=1, concat_axis=0, tiled=True)
    width = residual.shape[1]
    features = width * sp_count
    for layer_index in range(LAYERS):
        wide = residual.astype(jnp.float32)
        squares = lax.psum_scatter(
            jnp.sum(wide * wide, axis=-1, keepdims=True), "sp", scatter_dimension=0, tiled=True
        )
        inverse = lax.rsqrt(squares / features + norm_eps)
        gain = lax.dynamic_slice_in_dim(norm_gain[layer_index], sp_index * width, width, 0)
        gained = (wide * gain.astype(jnp.float32)).astype(jnp.bfloat16)
        partial = jnp.dot(gained, qkv_weight[layer_index], preferred_element_type=jnp.float32)
        mine = lax.psum_scatter(
            partial.astype(jnp.bfloat16), "sp", scatter_dimension=0, tiled=True
        )
        mine = (mine.astype(jnp.float32) * inverse).astype(jnp.bfloat16)
        queries = mine[:, :head_width].reshape(local_rows, GRID_W, heads_here, HD)
        key_values = mine[:, head_width:].reshape(local_rows, GRID_W, 2 * head_width)
        padded = with_halo(key_values, (("sp", 0),), reach)
        bands = jax.vmap(lambda band_begin: lax.dynamic_slice_in_dim(padded, band_begin, KR, 0))(
            band_start
        )
        band_keys = bands[..., :head_width].reshape(local_rows, KR, GRID_W, heads_here, HD)
        band_values = bands[..., head_width:].reshape(local_rows, KR, GRID_W, heads_here, HD)
        col_bias = jnp.einsum(
            "hro,oqk->hrqk", offset_bias[layer_index], col_onehot, precision=lax.Precision.HIGHEST
        )
        full_bias = jnp.einsum(
            "ijr,hrqk->hiqjk", row_onehot, col_bias, precision=lax.Precision.HIGHEST
        )
        scores = jnp.einsum(
            "iqhd,ijkhd->hiqjk", queries, band_keys, preferred_element_type=jnp.float32
        )
        scores = scores * scale + full_bias
        scores = jnp.where(col_inside[None, None, :, None, :], scores, -jnp.inf)
        flattened = scores.reshape(heads_here, local_rows, GRID_W, KR * GRID_W)
        weights = jax.nn.softmax(flattened, axis=-1).astype(jnp.bfloat16)
        weights = weights.reshape(heads_here, local_rows, GRID_W, KR, GRID_W)
        attended = jnp.einsum(
            "hiqjk,ijkhd->iqhd", weights, band_values, preferred_element_type=jnp.float32
        )
        attended = attended.astype(jnp.bfloat16).reshape(tok_rows, head_width)
        every = lax.all_gather(attended, "sp", axis=0, tiled=True)
        share = jnp.dot(every, w_out[layer_index], preferred_element_type=jnp.float32)
        branch = lax.psum(share.astype(jnp.bfloat16), "tp").astype(jnp.float32)
        residual = (residual.astype(jnp.float32) + branch).astype(jnp.bfloat16)
    return lax.all_to_all(residual, "sp", split_axis=0, concat_axis=1, tiled=True)


MESH = pl.DeviceIdType.MESH
VMEM_MOST = 63 * 2**20
CHUNK = GRID_W
HOP = 2
LEAD = 4


def greet(peers):
    barrier = pltpu.get_barrier_semaphore()
    for axis, index in peers:
        pl.semaphore_signal(barrier, inc=1, device_id={axis: index}, device_id_type=MESH)
    pl.semaphore_wait(barrier, len(peers))


def remote(src, dst, send, recv, axis, index):
    return pltpu.make_async_remote_copy(
        src_ref=src, dst_ref=dst, send_sem=send, recv_sem=recv,
        device_id={axis: index}, device_id_type=MESH,
    )


def span(start, size):
    return pl.ds(pl.multiple_of(start, size), size)


def row_plan(count, last):
    if not last:
        return [(r, 1) for r in range(count)]
    need = [min(max(r + KR - 1 - KR // 2, KR - 1), count - 1) - KR + 1 for r in range(count)]
    plan, done = [], 0
    for tick in range(need[-1] + 1):
        ready = sum(v <= tick for v in need) - done
        take = ready if tick == need[-1] else min(ready, 2)
        plan.append((done, take))
        done += take
    return plan


def pick(table, index):
    value = jnp.int32(table[-1])
    for i in range(len(table) - 2, -1, -1):
        value = jnp.where(index <= i, jnp.int32(table[i]), value)
    return value


def pipeline_kernel(
    n, m, tok_ref, gain_ref, base_ref, wq_any, wk_any, wv_any, wo_any, out_ref,
    wq, wk, wv, wo, xs, part, outbox, inbox, qkv, bias, sq_own, sq_in, box,
    give, take, pair, cross_in, fin,
    w_sem, sp_s, sp_r, spx_s, spx_r, fresh_s, fresh_r, ch_s, ch_r, sq_s, sq_r,
    at_s, at_r, gv_s, gv_r, cr_s, cr_r, fin_s, fin_r, fx_s, fx_r, fp_s, fp_r,
):
    me, t = lax.axis_index("sp"), lax.axis_index("tp")
    core = lax.rem(t, 2)
    side = lax.div(t, 2)
    partner = t + 1 - 2 * core
    cross = lax.rem(t + m // 2, m)
    layers, tokens, width = xs.shape
    own, features = tok_ref.shape
    cols = box.shape[3]
    heads = cols // HD
    half, quarter = width // 2, width // 4
    count, per = tokens // CHUNK, own // CHUNK
    scale = HD ** (-0.5)
    at_end = (me == 0) | (me == n - 1)
    ends = (n - 1, 0)
    lanes = span(core * half, half)
    other = span((1 - core) * half, half)
    mine_q = core * half + side * quarter
    their_q = core * half + (1 - side) * quarter
    places = (me, n - 1 - me)
    afters = (me + 1, me - 1)

    weights = []
    for layer in range(layers):
        for i, (any_ref, ref) in enumerate(((wq_any, wq), (wk_any, wk), (wv_any, wv), (wo_any, wo))):
            copy = pltpu.make_async_copy(any_ref.at[layer], ref.at[layer], w_sem.at[layer, i])
            copy.start()
            weights.append(copy)
    greet(
        [("sp", lax.rem(me + k, n)) for k in range(1, n)] + [("tp", partner), ("tp", cross)]
    )

    def rows_of(c):
        return span(c * CHUNK, CHUNK)

    def scatter(c):
        @pl.when(lax.div(c, per) == me)
        def _():
            here = span((c - me * per) * CHUNK, CHUNK)
            for k in range(1, n):
                to = lax.rem(me + k, n)
                remote(
                    tok_ref.at[here, span(to * width + mine_q, quarter)],
                    xs.at[0, rows_of(c), span(mine_q, quarter)],
                    sp_s, sp_r.at[c], "sp", to,
                ).start()
            xs[0, rows_of(c), :] = tok_ref[here, span(me * width, width)]

    def pass_cross(c):
        @pl.when(lax.div(c, per) != me)
        def _():
            here = xs.at[0, rows_of(c), span(mine_q, quarter)]
            remote(here, here, sp_s, sp_r.at[c], "tp", cross).wait_recv()
            remote(here, here, spx_s, spx_r.at[c], "tp", cross).start()

    def pass_partner(c):
        @pl.when(lax.div(c, per) != me)
        def _():
            there = xs.at[0, rows_of(c), span(their_q, quarter)]
            remote(there, there, spx_s, spx_r.at[c], "tp", cross).wait_recv()
            here = xs.at[0, rows_of(c), lanes]
            remote(here, here, fresh_s.at[0], fresh_r.at[0, c], "tp", partner).start()

    def prepare(layer, c):
        rows = rows_of(c)

        def arrived():
            there = xs.at[layer, rows, other]
            remote(there, there, fresh_s.at[layer], fresh_r.at[layer, c], "tp", partner).wait_recv()

        if layer == 0:
            pl.when(lax.div(c, per) != me)(arrived)
        else:
            arrived()
        gain = gain_ref[layer:layer + 1, span(me * width, width)].astype(jnp.float32)
        wide = xs[layer, rows, :].astype(jnp.float32)
        gained = (wide * gain).astype(jnp.bfloat16)
        for way in range(2):
            lo = (1 - way) * cols
            for j, w_ref in enumerate((wq, wk, wv)):
                part[way, rows, j * cols:(j + 1) * cols] = jnp.dot(
                    gained, w_ref[layer, :, lo:lo + cols], preferred_element_type=jnp.float32
                )
        squares = wide * wide
        high = squares.astype(jnp.bfloat16)
        low = (squares - high.astype(jnp.float32)).astype(jnp.bfloat16)
        ones = jnp.ones((8, width), jnp.bfloat16)
        nt = (((1,), (1,)), ((), ()))
        total = lax.dot_general(
            ones, high, nt, preferred_element_type=jnp.float32
        ) + lax.dot_general(ones, low, nt, preferred_element_type=jnp.float32)
        sq_own[layer, c] = jnp.concatenate([total] * (128 // CHUNK), axis=1)
        for e, end in enumerate(ends):
            @pl.when(me != end)
            def _(e=e, end=end):
                remote(
                    sq_own.at[layer, c], sq_in.at[layer, me, c],
                    sq_s.at[layer, e], sq_r.at[layer, me, c], "sp", end,
                ).start()

    def chain_copy(layer, way, c):
        rows = rows_of(c)
        return remote(
            outbox.at[layer, way, rows, :], inbox.at[layer, way, rows, :],
            ch_s.at[layer, way], ch_r.at[layer, way, c], "sp", afters[way],
        )

    def first_link(layer, c):
        for way in range(2):
            @pl.when(places[way] == 0)
            def _(way=way):
                outbox[layer, way, rows_of(c), :] = part[way, rows_of(c), :].astype(jnp.bfloat16)
                chain_copy(layer, way, c).start()

    def link(way, layer, c):
        rows = rows_of(c)
        place = places[way]
        chain_copy(layer, way, c).wait_recv()

        def total():
            return part[way, rows, :] + inbox[layer, way, rows, :].astype(jnp.float32)

        @pl.when(place < n - 1)
        def _():
            outbox[layer, way, rows, :] = total().astype(jnp.bfloat16)
            chain_copy(layer, way, c).start()

        @pl.when(place == n - 1)
        def _():
            squares = sq_own[layer, c]
            for k in range(1, n):
                source = lax.rem(me + k, n)
                remote(
                    sq_own.at[layer, c], sq_in.at[layer, source, c],
                    sq_s.at[layer, 0], sq_r.at[layer, source, c], "sp", source,
                ).wait_recv()
                squares = squares + sq_in[layer, source, c]
            scaled = lax.rsqrt(squares / features + norm_eps)
            inverse = jnp.concatenate([scaled] * 16, axis=0).T[:CHUNK, :1]
            qkv[layer, rows, :] = (total() * inverse).astype(jnp.bfloat16)

    def make_bias():
        first_head = jnp.where(me == n - 1, heads, 0)
        lane = lax.broadcasted_iota(jnp.int32, (CHUNK, 2 * GRID_W), 1)
        query = lax.broadcasted_iota(jnp.int32, (CHUNK, 2 * GRID_W), 0)
        key = jnp.where(lane < GRID_W, lane, lane - GRID_W)
        begin = jnp.clip(query - KC // 2, 0, GRID_W - KC)
        inside = (key >= begin) & (key < begin + KC)
        for layer in range(layers):
            for h in range(heads):
                @pl.loop(0, 2 * KR - 2)
                def _(o):
                    def rolled(i, shift):
                        row = base_ref[layer, first_head + h, pl.ds(i, 1), :]
                        return pltpu.roll(
                            jnp.broadcast_to(row, (CHUNK, 2 * GRID_W)), shift, 1, stride=1, stride_axis=0
                        )

                    both = jnp.where(lane < GRID_W, rolled(o, 0), rolled(o + 1, GRID_W))
                    bias[layer, h, o] = jnp.where(inside, both, -jnp.inf)

    way_here = jnp.where(me == 0, 0, 1)
    after_here = jnp.where(me == 0, 1, n - 2)

    def attend(layer, r):
        @pl.when(at_end)
        def _():
            first = jnp.clip(r - KR // 2, 0, count - KR)
            a = first - r + KR - 1
            rows = rows_of(r)
            band = pl.ds(pl.multiple_of(first * CHUNK, CHUNK), KR * CHUNK)
            outs = []
            for h in range(heads):
                at = [j * cols + h * HD for j in range(3)]
                q = qkv[layer, rows, at[0]:at[0] + HD]
                k = qkv[layer, band, at[1]:at[1] + HD]
                v = qkv[layer, band, at[2]:at[2] + HD]
                scores = lax.dot_general(
                    q, k, (((1,), (1,)), ((), ())), preferred_element_type=jnp.float32
                )
                table = jnp.concatenate([bias[layer, h, a + 2 * i] for i in range(KR // 2)], axis=1)
                scores = scores * scale + table
                scores = jnp.exp(scores - jnp.max(scores, axis=-1, keepdims=True))
                total = jnp.sum(scores, axis=-1, keepdims=True)
                out = jnp.dot(scores.astype(jnp.bfloat16), v, preferred_element_type=jnp.float32)
                outs.append(out / total)
            box[layer, way_here, rows, :] = jnp.concatenate(outs, axis=1).astype(jnp.bfloat16)
            here = box.at[layer, way_here, rows, :]
            remote(
                here, here, at_s.at[layer, way_here], at_r.at[layer, way_here, r], "sp", after_here
            ).start()

    def box_copy(layer, way, r):
        here = box.at[layer, way, rows_of(r), :]
        return remote(here, here, at_s.at[layer, way], at_r.at[layer, way, r], "sp", afters[way])

    def relay(way, layer, r):
        box_copy(layer, way, r).wait_recv()
        box_copy(layer, way, r).start()

    def give_copy(layer, r):
        rows = rows_of(r)
        return remote(
            give.at[layer, rows, :], take.at[layer, rows, :],
            gv_s.at[layer], gv_r.at[layer, r], "tp", partner,
        )

    def cross_copy(layer, r):
        rows = rows_of(r)
        return remote(
            pair.at[layer, rows, :], cross_in.at[layer, rows, :],
            cr_s.at[layer], cr_r.at[layer, r], "tp", cross,
        )

    def multiply(layer, r):
        for way in range(2):
            @pl.when(places[way] == n - 1)
            def _(way=way):
                box_copy(layer, way, r).wait_recv()
        rows = rows_of(r)

        def share(at):
            return jnp.dot(
                box[layer, 0, rows, :], wo[layer, :cols, at], preferred_element_type=jnp.float32
            ) + jnp.dot(box[layer, 1, rows, :], wo[layer, cols:, at], preferred_element_type=jnp.float32)

        give[layer, rows, :] = share(other).astype(jnp.bfloat16)
        give_copy(layer, r).start()
        pair[layer, rows, :] = share(lanes).astype(jnp.bfloat16)

    def meet(layer, r):
        rows = rows_of(r)
        give_copy(layer, r).wait_recv()
        pair[layer, rows, :] = (
            pair[layer, rows, :].astype(jnp.float32) + take[layer, rows, :].astype(jnp.float32)
        ).astype(jnp.bfloat16)
        cross_copy(layer, r).start()

    def out_at(q, lane, size):
        return out_ref.at[span(q * CHUNK, CHUNK), span(lane, size)]

    def finish(layer, r):
        rows = rows_of(r)
        cross_copy(layer, r).wait_recv()

        def new(at, sub):
            branch = pair[layer, rows, sub].astype(jnp.float32) + cross_in[layer, rows, sub].astype(jnp.float32)
            return (xs[layer, rows, at].astype(jnp.float32) + branch).astype(jnp.bfloat16)

        if layer < layers - 1:
            here = xs.at[layer + 1, rows, lanes]
            here[...] = new(lanes, slice(None))
            remote(here, here, fresh_s.at[layer + 1], fresh_r.at[layer + 1, r], "tp", partner).start()
            return
        owner, q = lax.div(r, per), lax.rem(r, per)

        @pl.when(owner == me)
        def _():
            here = out_at(q, me * width + core * half, half)
            here[...] = new(lanes, slice(None))
            remote(here, here, fp_s, fp_r.at[me, q], "tp", partner).start()

        @pl.when(owner != me)
        def _():
            fin[rows, :] = new(span(mine_q, quarter), span(side * quarter, quarter))
            remote(
                fin.at[rows, :], out_at(q, me * width + mine_q, quarter),
                fin_s, fin_r.at[me, q], "sp", owner,
            ).start()

    def hand_cross(layer, r):
        owner, q = lax.div(r, per), lax.rem(r, per)

        @pl.when(owner == me)
        def _():
            for k in range(1, n):
                source = lax.rem(me + k, n)
                here = out_at(q, source * width + mine_q, quarter)
                remote(here, here, fin_s, fin_r.at[source, q], "sp", source).wait_recv()
                remote(here, here, fx_s, fx_r.at[source, q], "tp", cross).start()

    def hand_partner(layer, r):
        owner, q = lax.div(r, per), lax.rem(r, per)

        @pl.when(owner == me)
        def _():
            for k in range(1, n):
                source = lax.rem(me + k, n)
                there = out_at(q, source * width + their_q, quarter)
                remote(there, there, fx_s, fx_r.at[source, q], "tp", cross).wait_recv()
                here = out_at(q, source * width + core * half, half)
                remote(here, here, fp_s, fp_r.at[source, q], "tp", partner).start()

    through = (n - 1) * HOP
    settle = n + 4
    starts = [layer * (through + KR - 1 + settle) for layer in range(layers)]
    plans = [row_plan(count, layer == layers - 1) for layer in range(layers)]
    final = starts[-1] + through + KR - 1 + len(plans[-1]) + n + 6

    @pl.loop(-LEAD, final)
    def _(tick):
        def chunks(stage, late, layer, extra=True):
            c = tick - late - starts[layer]

            @pl.when((c >= 0) & (c < count) & extra)
            def _():
                stage(layer, c)

        def grid_rows(stage, late, layer, extra=True):
            j = tick - late - starts[layer] - through - (KR - 1)
            plan = plans[layer]

            @pl.when((j >= 0) & (j < len(plan)) & extra)
            def _():
                if all(size == 1 for _, size in plan):
                    stage(layer, j)
                    return
                first, size = pick([p[0] for p in plan], j), pick([p[1] for p in plan], j)

                @pl.loop(first, first + size)
                def _(r):
                    stage(layer, r)

        @pl.when(tick == 0)
        def _():
            for copy in weights:
                copy.wait()

        for layer in range(layers):
            for way in range(2):
                inner = (places[way] > 0) & (places[way] < n - 1)
                grid_rows(functools.partial(relay, way), 1 + places[way], layer, inner)
        for layer in range(layers):
            for way in range(2):
                chunks(functools.partial(link, way), HOP * places[way], layer, places[way] > 0)
        grid_rows(hand_partner, n + 6, layers - 1)
        grid_rows(hand_cross, n + 5, layers - 1)
        for layer in range(layers):
            grid_rows(finish, n + 3, layer)
            grid_rows(meet, n + 1, layer)
            grid_rows(multiply, n, layer)

        chunks(lambda _, c: pass_partner(c), -1, 0)
        chunks(lambda _, c: pass_cross(c), -2, 0)
        chunks(lambda _, c: scatter(c), -LEAD, 0)

        @pl.when((tick == 1 - LEAD) & at_end)
        def _():
            make_bias()

        for layer in range(layers):
            chunks(prepare, jnp.where(at_end, 0, HOP - 1), layer)
            chunks(first_link, 0, layer, at_end)
        for layer in range(layers):
            grid_rows(attend, 0, layer)

    for q in range(per):
        for source in range(n):
            there = out_at(q, source * width + (1 - core) * half, half)
            remote(there, there, fp_s, fp_r.at[source, q], "tp", partner).wait_recv()

    def sent(ref, sem, recv):
        remote(ref, ref, sem, recv, "tp", partner).wait_send()

    away = fin.at[0:tokens - own, :]
    sent(away, sp_s, sp_r.at[0])
    sent(away, spx_s, spx_r.at[0])
    sent(away, fin_s, fin_r.at[0, 0])
    sent(away, fx_s, fx_r.at[0, 0])
    sent(xs.at[0, :, 0:half], fp_s, fp_r.at[0, 0])
    sent(xs.at[0, 0:tokens - own, 0:half], fresh_s.at[0], fresh_r.at[0, 0])
    for layer in range(layers):
        if layer > 0:
            sent(xs.at[layer, :, 0:half], fresh_s.at[layer], fresh_r.at[layer, 0])
        sent(give.at[layer], gv_s.at[layer], gv_r.at[layer, 0])
        sent(pair.at[layer], cr_s.at[layer], cr_r.at[layer, 0])
        for way in range(2):
            @pl.when(places[way] < n - 1)
            def _(way=way):
                sent(outbox.at[layer, way], ch_s.at[layer, way], ch_r.at[layer, way, 0])
                sent(box.at[layer, way], at_s.at[layer, way], at_r.at[layer, way, 0])

            @pl.when(me != ends[way])
            def _(way=way):
                sent(sq_own.at[layer], sq_s.at[layer, way], sq_r.at[layer, 0, 0])


def staged(tokens, norm_gain, w_query, w_key, w_value, w_out, offset_bias):
    n, m = lax.axis_size("sp"), lax.axis_size("tp")
    own, features = tokens.shape
    layers = norm_gain.shape[0]
    width, total = features // n, own * n
    heads = offset_bias.shape[1] // 2
    cols = heads * HD
    count, per = total // CHUNK, own // CHUNK
    dma = pltpu.SemaphoreType.DMA
    bf16, f32 = jnp.bfloat16, jnp.float32
    gap = jnp.zeros((*offset_bias.shape[:3], 2 * GRID_W - 2 * KC + 1), f32)
    base = jnp.concatenate([offset_bias[..., KC - 1:], gap, offset_bias[..., :KC - 1]], axis=-1)
    base = jnp.pad(base, ((0, 0), (0, 0), (0, 1), (0, 0)))
    space = pltpu.VMEM
    whole, anywhere = pl.BlockSpec(memory_space=space), pl.BlockSpec(memory_space=pl.ANY)
    return pl.pallas_call(
        functools.partial(pipeline_kernel, n, m),
        out_shape=jax.ShapeDtypeStruct((own, features), bf16),
        in_specs=[whole] * 3 + [anywhere] * 4,
        out_specs=whole,
        scratch_shapes=[
            *[space(w.shape, bf16) for w in (w_query, w_key, w_value, w_out)],
            space((layers, total, width), bf16),
            space((2, total, 3 * cols), f32),
            space((layers, 2, total, 3 * cols), bf16),
            space((layers, 2, total, 3 * cols), bf16),
            space((layers, total, 3 * cols), bf16),
            space((layers, heads, 2 * KR - 2, CHUNK, 2 * GRID_W), f32),
            space((layers, count, 8, 128), f32),
            space((layers, n, count, 8, 128), f32),
            space((layers, 2, total, cols), bf16),
            *[space((layers, total, width // 2), bf16)] * 4,
            space((total, width // 4), bf16),
            dma((layers, 4)),
            dma, dma((count,)), dma, dma((count,)), dma((layers,)), dma((layers, count)),
            dma((layers, 2)), dma((layers, 2, count)), dma((layers, 2)), dma((layers, n, count)),
            dma((layers, 2)), dma((layers, 2, count)),
            dma((layers,)), dma((layers, count)), dma((layers,)), dma((layers, count)),
            dma, dma((n, per)), dma, dma((n, per)), dma, dma((n, per)),
        ],
        compiler_params=pltpu.CompilerParams(
            collective_id=1, has_side_effects=True, vmem_limit_bytes=VMEM_MOST
        ),
        name="pipeline",
    )(tokens, norm_gain, base, w_query, w_key, w_value, w_out)


def on_device(tokens, norm_gain, w_query, w_key, w_value, w_out, offset_bias):
    n, m = lax.axis_size("sp"), lax.axis_size("tp")
    own, features = tokens.shape
    total, width = own * n, features // n
    fits = total * (20 * width + 60 * w_query.shape[2]) < VMEM_MOST
    even = offset_bias.shape[1] % 2 == 0 and m == 4 and n > 2
    if fits and even and own % CHUNK == 0 and width % 512 == 0 and total >= KR * GRID_W:
        return staged(tokens, norm_gain, w_query, w_key, w_value, w_out, offset_bias)
    return general(tokens, norm_gain, w_query, w_key, w_value, w_out, offset_bias)


def solution(mesh):
    return jax.shard_map(
        on_device,
        mesh=mesh,
        in_specs=(
            P(("grp", "sp"), None),
            P(),
            P(None, "sp", "tp"),
            P(None, "sp", "tp"),
            P(None, "sp", "tp"),
            P(None, "tp", "sp"),
            P(None, "tp", None, None),
        ),
        out_specs=P(("grp", "sp"), None),
        check_vma=False,
    )
```

time: 334 us -> 203 us (0.61)
  Pallas kernels: 307 us -> 197 us
  local copies, waits for them, and re-layouts: 18.3 us -> 5.61 us
  matrix products: 5.63 us -> 0 us
    pallas_call x7 -> x1, Pallas kernels: 307 us -> 197 us  [staged(): pl.pallas_call(functools.partial(pipeline_kernel, n, m), out_shape=jax.Sh...]
    reshape x2 -> x0, local copies, waits for them, and re-layouts: 14 us -> none  [staged(): bias = bias.reshape(LAYERS, heads, KR, GRID_W, KR * GRID_W)]
    dot_general x1 -> x0, matrix products: 5.63 us -> none  [staged(): jnp.einsum('lhajo,oqk->lhaqjk', table, onehot, precision=lax.Precision.HI...]
where the time goes in v1:
time: 203 us
  Pallas kernels  197 us (97%)
  local copies, waits for them, and re-layouts  5.61 us (3%)
    pallas_call x1, Pallas kernels, staged(): pl.pallas_call(functools.partial(pipeline_kernel, n, m), out_shape=jax.Sh...  197 us

profile of v1, /device:TPU:29, one launch (start us, length us, event | category | flops | bytes accessed | tf_op | source)
XLA Modules:
  0.0 202.7 jit_solution(14914198392075219862)
XLA Ops:
  0.0 0.1 pad.6.clone
  0.1 0.9 slice.6
  1.0 0.8 copy.11
  1.9 0.1 pad_maximum_fusion
  1.9 0.6 pad.4.base_ref
  2.6 197.0 %pipeline.1 = bf16[256,4096]{1,0:T(8,128)(2,1)} custom-call(bf16[256,4096]{1,0:T(8,128)(2,1)} %tok_ref.1, bf16[2,4096]{1,0:T(2,128)(2,1)} %gain_ref.1, f32[2,4,16,128]{3,2,1,0:T(8,128)} %pad.4.base_ref, bf16[2,1024,512]{2,1,0:T(8,128)(2,1)} %wq_any.1, bf16[2,1024,512]{2,1,0:T(8,128)(2,1)} %wk_any.1, bf16[2,1024,512]{2,1,0:T(8,128)(2,1)} %wv_any.1, ...), custom_call_target="tpu_custom_call" | custom-call | tf_op jit(solution)/shard_map/pipeline/pallas_call | solution.py:571
  199.6 3.1 %copy.13 = bf16[256,4096]{1,0:T(8,128)(2,1)} copy(bf16[256,4096]{1,0:T(8,128)(2,1)} %pipeline.1) | data formatting | bytes 4194304
  (2 shorter events, 0.0 us)

commit v2 on v1

--- a/solution.py
+++ b/solution.py
@@ -119,7 +119,11 @@
 VMEM_MOST = 63 * 2**20
 CHUNK = GRID_W
 HOP = 2
-LEAD = 4
+LEAD, OWN_LEAD, TURN, PASS = 6, 4, 2, 1
+PARTS = 3
+FIRST, RELAY = 2, 1
+MEET, CROSS, FRESH = 0, 2, 0
+HOLD = 6
 
 
 def greet(peers):
@@ -144,13 +148,11 @@
     if not last:
         return [(r, 1) for r in range(count)]
     need = [min(max(r + KR - 1 - KR // 2, KR - 1), count - 1) - KR + 1 for r in range(count)]
-    plan, done = [], 0
-    for tick in range(need[-1] + 1):
-        ready = sum(v <= tick for v in need) - done
-        take = ready if tick == need[-1] else min(ready, 2)
-        plan.append((done, take))
-        done += take
-    return plan
+    ticks = need[-1]
+    early = sum(v < ticks for v in need)
+    sizes = [early // ticks + (t >= ticks - early % ticks) for t in range(ticks)] + [count - early]
+    starts = [sum(sizes[:t]) for t in range(ticks + 1)]
+    return list(zip(starts, sizes))
 
 
 def pick(table, index):
@@ -206,7 +208,7 @@
         def _():
             here = span((c - me * per) * CHUNK, CHUNK)
             for k in range(1, n):
-                to = lax.rem(me + k, n)
+                to = jnp.where(me < n // 2, n - k + jnp.where(n - k > me, 0, -1), k - 1 + jnp.where(k > me, 1, 0))
                 remote(
                     tok_ref.at[here, span(to * width + mine_q, quarter)],
                     xs.at[0, rows_of(c), span(mine_q, quarter)],
@@ -266,32 +268,36 @@
                     sq_s.at[layer, e], sq_r.at[layer, me, c], "sp", end,
                 ).start()
 
-    def chain_copy(layer, way, c):
+    pieces = [slice(i * 3 * cols // PARTS, (i + 1) * 3 * cols // PARTS) for i in range(PARTS)]
+
+    def chain_copy(layer, way, c, i):
         rows = rows_of(c)
         return remote(
-            outbox.at[layer, way, rows, :], inbox.at[layer, way, rows, :],
-            ch_s.at[layer, way], ch_r.at[layer, way, c], "sp", afters[way],
+            outbox.at[layer, way, rows, pieces[i]], inbox.at[layer, way, rows, pieces[i]],
+            ch_s.at[layer, way], ch_r.at[layer, way, c, i], "sp", afters[way],
         )
 
     def first_link(layer, c):
         for way in range(2):
             @pl.when(places[way] == 0)
             def _(way=way):
-                outbox[layer, way, rows_of(c), :] = part[way, rows_of(c), :].astype(jnp.bfloat16)
-                chain_copy(layer, way, c).start()
+                for i, at in enumerate(pieces):
+                    outbox[layer, way, rows_of(c), at] = part[way, rows_of(c), at].astype(jnp.bfloat16)
+                    chain_copy(layer, way, c, i).start()
 
     def link(way, layer, c):
         rows = rows_of(c)
         place = places[way]
-        chain_copy(layer, way, c).wait_recv()
-
-        def total():
-            return part[way, rows, :] + inbox[layer, way, rows, :].astype(jnp.float32)
+
+        def total(i):
+            chain_copy(layer, way, c, i).wait_recv()
+            return part[way, rows, pieces[i]] + inbox[layer, way, rows, pieces[i]].astype(jnp.float32)
 
         @pl.when(place < n - 1)
         def _():
-            outbox[layer, way, rows, :] = total().astype(jnp.bfloat16)
-            chain_copy(layer, way, c).start()
+            for i, at in enumerate(pieces):
+                outbox[layer, way, rows, at] = total(i).astype(jnp.bfloat16)
+                chain_copy(layer, way, c, i).start()
 
         @pl.when(place == n - 1)
         def _():
@@ -305,9 +311,10 @@
                 squares = squares + sq_in[layer, source, c]
             scaled = lax.rsqrt(squares / features + norm_eps)
             inverse = jnp.concatenate([scaled] * 16, axis=0).T[:CHUNK, :1]
-            qkv[layer, rows, :] = (total() * inverse).astype(jnp.bfloat16)
-
-    def make_bias():
+            for i, at in enumerate(pieces):
+                qkv[layer, rows, at] = (total(i) * inverse).astype(jnp.bfloat16)
+
+    def make_bias(o):
         first_head = jnp.where(me == n - 1, heads, 0)
         lane = lax.broadcasted_iota(jnp.int32, (CHUNK, 2 * GRID_W), 1)
         query = lax.broadcasted_iota(jnp.int32, (CHUNK, 2 * GRID_W), 0)
@@ -316,16 +323,14 @@
         inside = (key >= begin) & (key < begin + KC)
         for layer in range(layers):
             for h in range(heads):
-                @pl.loop(0, 2 * KR - 2)
-                def _(o):
-                    def rolled(i, shift):
-                        row = base_ref[layer, first_head + h, pl.ds(i, 1), :]
-                        return pltpu.roll(
-                            jnp.broadcast_to(row, (CHUNK, 2 * GRID_W)), shift, 1, stride=1, stride_axis=0
-                        )
-
-                    both = jnp.where(lane < GRID_W, rolled(o, 0), rolled(o + 1, GRID_W))
-                    bias[layer, h, o] = jnp.where(inside, both, -jnp.inf)
+                def rolled(i, shift, layer=layer, h=h):
+                    row = base_ref[layer, first_head + h, pl.ds(i, 1), :]
+                    return pltpu.roll(
+                        jnp.broadcast_to(row, (CHUNK, 2 * GRID_W)), shift, 1, stride=1, stride_axis=0
+                    )
+
+                both = jnp.where(lane < GRID_W, rolled(o, 0), rolled(o + 1, GRID_W))
+                bias[layer, h, o] = jnp.where(inside, both, -jnp.inf)
 
     way_here = jnp.where(me == 0, 0, 1)
     after_here = jnp.where(me == 0, 1, n - 2)
@@ -374,9 +379,10 @@
         )
 
     def cross_copy(layer, r):
+        at = slice(None) if layer < layers - 1 else span((1 - side) * quarter, quarter)
         rows = rows_of(r)
         return remote(
-            pair.at[layer, rows, :], cross_in.at[layer, rows, :],
+            pair.at[layer, rows, at], cross_in.at[layer, rows, at],
             cr_s.at[layer], cr_r.at[layer, r], "tp", cross,
         )
 
@@ -421,49 +427,42 @@
             remote(here, here, fresh_s.at[layer + 1], fresh_r.at[layer + 1, r], "tp", partner).start()
             return
         owner, q = lax.div(r, per), lax.rem(r, per)
+        here = out_at(q, me * width + mine_q, quarter)
+        value = new(span(mine_q, quarter), span(side * quarter, quarter))
 
         @pl.when(owner == me)
         def _():
-            here = out_at(q, me * width + core * half, half)
-            here[...] = new(lanes, slice(None))
-            remote(here, here, fp_s, fp_r.at[me, q], "tp", partner).start()
+            here[...] = value
+            remote(here, here, fx_s, fx_r.at[me, q], "tp", cross).start()
 
         @pl.when(owner != me)
         def _():
-            fin[rows, :] = new(span(mine_q, quarter), span(side * quarter, quarter))
-            remote(
-                fin.at[rows, :], out_at(q, me * width + mine_q, quarter),
-                fin_s, fin_r.at[me, q], "sp", owner,
-            ).start()
-
-    def hand_cross(layer, r):
-        owner, q = lax.div(r, per), lax.rem(r, per)
-
-        @pl.when(owner == me)
-        def _():
-            for k in range(1, n):
-                source = lax.rem(me + k, n)
-                here = out_at(q, source * width + mine_q, quarter)
-                remote(here, here, fin_s, fin_r.at[source, q], "sp", source).wait_recv()
-                remote(here, here, fx_s, fx_r.at[source, q], "tp", cross).start()
-
-    def hand_partner(layer, r):
-        owner, q = lax.div(r, per), lax.rem(r, per)
-
-        @pl.when(owner == me)
-        def _():
-            for k in range(1, n):
-                source = lax.rem(me + k, n)
-                there = out_at(q, source * width + their_q, quarter)
-                remote(there, there, fx_s, fx_r.at[source, q], "tp", cross).wait_recv()
-                here = out_at(q, source * width + core * half, half)
-                remote(here, here, fp_s, fp_r.at[source, q], "tp", partner).start()
+            fin[rows, :] = value
+            remote(fin.at[rows, :], here, fin_s, fin_r.at[me, q], "sp", owner).start()
+
+    def hand_cross(q):
+        for k in range(1, n):
+            source = lax.rem(me + k, n)
+            here = out_at(q, source * width + mine_q, quarter)
+            remote(here, here, fin_s, fin_r.at[source, q], "sp", source).wait_recv()
+            remote(here, here, fx_s, fx_r.at[source, q], "tp", cross).start()
+
+    def hand_partner(q):
+        for k in range(n):
+            source = lax.rem(me + k, n)
+            there = out_at(q, source * width + their_q, quarter)
+            remote(there, there, fx_s, fx_r.at[source, q], "tp", cross).wait_recv()
+            here = out_at(q, source * width + core * half, half)
+            remote(here, here, fp_s, fp_r.at[source, q], "tp", partner).start()
 
     through = (n - 1) * HOP
-    settle = n + 4
+    share_at = FIRST + (n - 2) * RELAY
+    meet_at = share_at + MEET
+    finish_at = meet_at + CROSS
+    settle = finish_at + FRESH
     starts = [layer * (through + KR - 1 + settle) for layer in range(layers)]
     plans = [row_plan(count, layer == layers - 1) for layer in range(layers)]
-    final = starts[-1] + through + KR - 1 + len(plans[-1]) + n + 6
+    final = starts[-1] + through + KR - 1 + len(plans[-1]) + finish_at
 
     @pl.loop(-LEAD, final)
     def _(tick):
@@ -474,9 +473,9 @@
             def _():
                 stage(layer, c)
 
-        def grid_rows(stage, late, layer, extra=True):
+        def grid_rows(stage, late, layer, extra=True, plan=None):
             j = tick - late - starts[layer] - through - (KR - 1)
-            plan = plans[layer]
+            plan = plan or plans[layer]
 
             @pl.when((j >= 0) & (j < len(plan)) & extra)
             def _():
@@ -489,38 +488,55 @@
                 def _(r):
                     stage(layer, r)
 
+        def relays(low, high):
+            for layer in range(layers):
+                for way in range(2):
+                    place = places[way]
+                    inner = (place >= low) & (place < high)
+                    grid_rows(functools.partial(relay, way), FIRST + (place - 1) * RELAY, layer, inner)
+
         @pl.when(tick == 0)
         def _():
             for copy in weights:
                 copy.wait()
 
-        for layer in range(layers):
-            for way in range(2):
-                inner = (places[way] > 0) & (places[way] < n - 1)
-                grid_rows(functools.partial(relay, way), 1 + places[way], layer, inner)
+        last = layers - 1
+        relays(1, 2)
+        chunks(lambda _, c: pass_cross(c), -TURN, 0)
         for layer in range(layers):
             for way in range(2):
                 chunks(functools.partial(link, way), HOP * places[way], layer, places[way] > 0)
-        grid_rows(hand_partner, n + 6, layers - 1)
-        grid_rows(hand_cross, n + 5, layers - 1)
+        for layer in range(last):
+            grid_rows(finish, finish_at, layer)
+        held = plans[last][HOLD + 1:]
+        held = [(0, held[0][0])] + held
+        grid_rows(finish, finish_at + HOLD, last, plan=held)
         for layer in range(layers):
-            grid_rows(finish, n + 3, layer)
-            grid_rows(meet, n + 1, layer)
-            grid_rows(multiply, n, layer)
-
-        chunks(lambda _, c: pass_partner(c), -1, 0)
-        chunks(lambda _, c: pass_cross(c), -2, 0)
-        chunks(lambda _, c: scatter(c), -LEAD, 0)
-
-        @pl.when((tick == 1 - LEAD) & at_end)
-        def _():
-            make_bias()
+            grid_rows(attend, 0, layer)
+        relays(2, n - 1)
+        for layer in range(layers):
+            grid_rows(multiply, share_at, layer)
+
+        chunks(lambda _, c: pass_partner(c), -PASS, 0)
+        chunks(lambda _, c: scatter(c), -jnp.where(me == 0, OWN_LEAD, LEAD), 0)
+
+        @pl.when((tick >= -1) & (tick < 2 * KR - 3) & at_end)
+        def _():
+            make_bias(tick + 1)
 
         for layer in range(layers):
             chunks(prepare, jnp.where(at_end, 0, HOP - 1), layer)
             chunks(first_link, 0, layer, at_end)
         for layer in range(layers):
-            grid_rows(attend, 0, layer)
+            grid_rows(meet, meet_at, layer)
+
+    @pl.loop(0, per)
+    def _(q):
+        hand_cross(q)
+
+    @pl.loop(0, per)
+    def _(q):
+        hand_partner(q)
 
     for q in range(per):
         for source in range(n):
@@ -534,18 +550,19 @@
     sent(away, sp_s, sp_r.at[0])
     sent(away, spx_s, spx_r.at[0])
     sent(away, fin_s, fin_r.at[0, 0])
-    sent(away, fx_s, fx_r.at[0, 0])
+    sent(fin, fx_s, fx_r.at[0, 0])
     sent(xs.at[0, :, 0:half], fp_s, fp_r.at[0, 0])
     sent(xs.at[0, 0:tokens - own, 0:half], fresh_s.at[0], fresh_r.at[0, 0])
     for layer in range(layers):
         if layer > 0:
             sent(xs.at[layer, :, 0:half], fresh_s.at[layer], fresh_r.at[layer, 0])
         sent(give.at[layer], gv_s.at[layer], gv_r.at[layer, 0])
-        sent(pair.at[layer], cr_s.at[layer], cr_r.at[layer, 0])
+        swapped = pair.at[layer] if layer < layers - 1 else pair.at[layer, :, 0:quarter]
+        sent(swapped, cr_s.at[layer], cr_r.at[layer, 0])
         for way in range(2):
             @pl.when(places[way] < n - 1)
             def _(way=way):
-                sent(outbox.at[layer, way], ch_s.at[layer, way], ch_r.at[layer, way, 0])
+                sent(outbox.at[layer, way], ch_s.at[layer, way], ch_r.at[layer, way, 0, 0])
                 sent(box.at[layer, way], at_s.at[layer, way], at_r.at[layer, way, 0])
 
             @pl.when(me != ends[way])
@@ -588,7 +605,7 @@
             space((total, width // 4), bf16),
             dma((layers, 4)),
             dma, dma((count,)), dma, dma((count,)), dma((layers,)), dma((layers, count)),
-            dma((layers, 2)), dma((layers, 2, count)), dma((layers, 2)), dma((layers, n, count)),
+            dma((layers, 2)), dma((layers, 2, count, PARTS)), dma((layers, 2)), dma((layers, n, count)),
             dma((layers, 2)), dma((layers, 2, count)),
             dma((layers,)), dma((layers, count)), dma((layers,)), dma((layers, count)),
             dma, dma((n, per)), dma, dma((n, per)), dma, dma((n, per)),

time: 203 us -> 184 us (0.906)
  Pallas kernels: 197 us -> 177 us
    pallas_call x1, Pallas kernels: 197 us -> 177 us  [staged(): pl.pallas_call(functools.partial(pipeline_kernel, n, m), out_shape=jax.Sh...]
where the time goes in v2:
time: 184 us; the launch traced here: 182 us
  Pallas kernels  177 us (96%)
  local copies, waits for them, and re-layouts  5.61 us (3%)
    pallas_call x1, Pallas kernels, staged(): pl.pallas_call(functools.partial(pipeline_kernel, n, m), out_shape=jax.Sh...  177 us
    unnamed x3, local copies, waits for them, and re-layouts  3.98 us

profile of v2, /device:TPU:29, one launch (start us, length us, event | category | flops | bytes accessed | tf_op | source)
XLA Modules:
  0.0 182.5 jit_solution(3393390875123129692)
XLA Ops:
  0.0 0.1 pad.6.clone
  0.1 0.9 slice.6
  1.0 0.8 copy.11
  1.9 0.1 pad_maximum_fusion
  1.9 0.6 pad.4.base_ref
  2.6 176.8 %pipeline.1 = bf16[256,4096]{1,0:T(8,128)(2,1)} custom-call(bf16[256,4096]{1,0:T(8,128)(2,1)} %tok_ref.1, bf16[2,4096]{1,0:T(2,128)(2,1)} %gain_ref.1, f32[2,4,16,128]{3,2,1,0:T(8,128)} %pad.4.base_ref, bf16[2,1024,512]{2,1,0:T(8,128)(2,1)} %wq_any.1, bf16[2,1024,512]{2,1,0:T(8,128)(2,1)} %wk_any.1, bf16[2,1024,512]{2,1,0:T(8,128)(2,1)} %wv_any.1, ...), custom_call_target="tpu_custom_call" | custom-call | tf_op jit(solution)/shard_map/pipeline/pallas_call | solution.py:588
  179.4 3.1 %copy.13 = bf16[256,4096]{1,0:T(8,128)(2,1)} copy(bf16[256,4096]{1,0:T(8,128)(2,1)} %pipeline.1) | data formatting | bytes 4194304
  (2 shorter events, 0.0 us)

commit v3 on v2

--- a/solution.py
+++ b/solution.py
@@ -116,7 +116,7 @@
 
 
 MESH = pl.DeviceIdType.MESH
-VMEM_MOST = 63 * 2**20
+VMEM_MOST = 56 * 2**20
 CHUNK = GRID_W
 HOP = 2
 LEAD, OWN_LEAD, TURN, PASS = 6, 4, 2, 1
@@ -124,6 +124,7 @@
 FIRST, RELAY = 2, 1
 MEET, CROSS, FRESH = 0, 2, 0
 HOLD = 6
+FAR_FIRST = True
 
 
 def greet(peers):
@@ -163,9 +164,9 @@
 
 
 def pipeline_kernel(
-    n, m, tok_ref, gain_ref, base_ref, wq_any, wk_any, wv_any, wo_any, out_ref,
+    n, m, tok_ref, gain_ref, offset_ref, wq_any, wk_any, wv_any, wo_any, out_ref,
     wq, wk, wv, wo, xs, part, outbox, inbox, qkv, bias, sq_own, sq_in, box,
-    give, take, pair, cross_in, fin,
+    give, take, pair, cross_in, fin, padded,
     w_sem, sp_s, sp_r, spx_s, spx_r, fresh_s, fresh_r, ch_s, ch_r, sq_s, sq_r,
     at_s, at_r, gv_s, gv_r, cr_s, cr_r, fin_s, fin_r, fx_s, fx_r, fp_s, fp_r,
 ):
@@ -229,14 +230,14 @@
             there = xs.at[0, rows_of(c), span(their_q, quarter)]
             remote(there, there, spx_s, spx_r.at[c], "tp", cross).wait_recv()
             here = xs.at[0, rows_of(c), lanes]
-            remote(here, here, fresh_s.at[0], fresh_r.at[0, c], "tp", partner).start()
+            remote(here, here, fresh_s.at[0], fresh_r.at[c], "tp", partner).start()
 
     def prepare(layer, c):
         rows = rows_of(c)
 
         def arrived():
             there = xs.at[layer, rows, other]
-            remote(there, there, fresh_s.at[layer], fresh_r.at[layer, c], "tp", partner).wait_recv()
+            remote(there, there, fresh_s.at[layer], fresh_r.at[c], "tp", partner).wait_recv()
 
         if layer == 0:
             pl.when(lax.div(c, per) != me)(arrived)
@@ -264,8 +265,8 @@
             @pl.when(me != end)
             def _(e=e, end=end):
                 remote(
-                    sq_own.at[layer, c], sq_in.at[layer, me, c],
-                    sq_s.at[layer, e], sq_r.at[layer, me, c], "sp", end,
+                    sq_own.at[layer, c], sq_in.at[layer, c, me],
+                    sq_s.at[layer, e], sq_r.at[c], "sp", end,
                 ).start()
 
     pieces = [slice(i * 3 * cols // PARTS, (i + 1) * 3 * cols // PARTS) for i in range(PARTS)]
@@ -274,7 +275,7 @@
         rows = rows_of(c)
         return remote(
             outbox.at[layer, way, rows, pieces[i]], inbox.at[layer, way, rows, pieces[i]],
-            ch_s.at[layer, way], ch_r.at[layer, way, c, i], "sp", afters[way],
+            ch_s.at[layer, way], ch_r.at[way, c, i], "sp", afters[way],
         )
 
     def first_link(layer, c):
@@ -302,13 +303,10 @@
         @pl.when(place == n - 1)
         def _():
             squares = sq_own[layer, c]
+            others = sq_in.at[layer, c, 0:n - 1]
+            remote(others, others, sq_s.at[layer, 0], sq_r.at[c], "sp", n - 1 - me).wait_recv()
             for k in range(1, n):
-                source = lax.rem(me + k, n)
-                remote(
-                    sq_own.at[layer, c], sq_in.at[layer, source, c],
-                    sq_s.at[layer, 0], sq_r.at[layer, source, c], "sp", source,
-                ).wait_recv()
-                squares = squares + sq_in[layer, source, c]
+                squares = squares + sq_in[layer, c, lax.rem(me + k, n)]
             scaled = lax.rsqrt(squares / features + norm_eps)
             inverse = jnp.concatenate([scaled] * 16, axis=0).T[:CHUNK, :1]
             for i, at in enumerate(pieces):
@@ -324,13 +322,22 @@
         for layer in range(layers):
             for h in range(heads):
                 def rolled(i, shift, layer=layer, h=h):
-                    row = base_ref[layer, first_head + h, pl.ds(i, 1), :]
+                    row = padded[layer, first_head + h, pl.ds(i, 1), :]
                     return pltpu.roll(
                         jnp.broadcast_to(row, (CHUNK, 2 * GRID_W)), shift, 1, stride=1, stride_axis=0
                     )
 
-                both = jnp.where(lane < GRID_W, rolled(o, 0), rolled(o + 1, GRID_W))
+                both = jnp.where(
+                    lane < GRID_W, rolled(o, 2 * GRID_W - KC + 1), rolled(o + 1, GRID_W - KC + 1)
+                )
                 bias[layer, h, o] = jnp.where(inside, both, -jnp.inf)
+
+    @pl.when(at_end)
+    def _():
+        padded[...] = jnp.zeros_like(padded)
+        for layer in range(layers):
+            for h in range(2 * heads):
+                padded[layer, h, 0:2 * KR - 1, 0:2 * KC - 1] = offset_ref[layer, h]
 
     way_here = jnp.where(me == 0, 0, 1)
     after_here = jnp.where(me == 0, 1, n - 2)
@@ -360,12 +367,12 @@
             box[layer, way_here, rows, :] = jnp.concatenate(outs, axis=1).astype(jnp.bfloat16)
             here = box.at[layer, way_here, rows, :]
             remote(
-                here, here, at_s.at[layer, way_here], at_r.at[layer, way_here, r], "sp", after_here
+                here, here, at_s.at[layer, way_here], at_r.at[way_here, r], "sp", after_here
             ).start()
 
     def box_copy(layer, way, r):
         here = box.at[layer, way, rows_of(r), :]
-        return remote(here, here, at_s.at[layer, way], at_r.at[layer, way, r], "sp", afters[way])
+        return remote(here, here, at_s.at[layer, way], at_r.at[way, r], "sp", afters[way])
 
     def relay(way, layer, r):
         box_copy(layer, way, r).wait_recv()
@@ -375,7 +382,7 @@
         rows = rows_of(r)
         return remote(
             give.at[layer, rows, :], take.at[layer, rows, :],
-            gv_s.at[layer], gv_r.at[layer, r], "tp", partner,
+            gv_s.at[layer], gv_r.at[r], "tp", partner,
         )
 
     def cross_copy(layer, r):
@@ -424,7 +431,7 @@
         if layer < layers - 1:
             here = xs.at[layer + 1, rows, lanes]
             here[...] = new(lanes, slice(None))
-            remote(here, here, fresh_s.at[layer + 1], fresh_r.at[layer + 1, r], "tp", partner).start()
+            remote(here, here, fresh_s.at[layer + 1], fresh_r.at[r], "tp", partner).start()
             return
         owner, q = lax.div(r, per), lax.rem(r, per)
         here = out_at(q, me * width + mine_q, quarter)
@@ -433,7 +440,7 @@
         @pl.when(owner == me)
         def _():
             here[...] = value
-            remote(here, here, fx_s, fx_r.at[me, q], "tp", cross).start()
+            remote(here, here, fx_s, fx_r.at[q], "tp", cross).start()
 
         @pl.when(owner != me)
         def _():
@@ -445,15 +452,14 @@
             source = lax.rem(me + k, n)
             here = out_at(q, source * width + mine_q, quarter)
             remote(here, here, fin_s, fin_r.at[source, q], "sp", source).wait_recv()
-            remote(here, here, fx_s, fx_r.at[source, q], "tp", cross).start()
+            remote(here, here, fx_s, fx_r.at[q], "tp", cross).start()
 
     def hand_partner(q):
-        for k in range(n):
-            source = lax.rem(me + k, n)
-            there = out_at(q, source * width + their_q, quarter)
-            remote(there, there, fx_s, fx_r.at[source, q], "tp", cross).wait_recv()
+        every = fin.at[0:n * CHUNK, :]
+        remote(every, every, fx_s, fx_r.at[q], "tp", cross).wait_recv()
+        for source in range(n):
             here = out_at(q, source * width + core * half, half)
-            remote(here, here, fp_s, fp_r.at[source, q], "tp", partner).start()
+            remote(here, here, fp_s, fp_r, "tp", partner).start()
 
     through = (n - 1) * HOP
     share_at = FIRST + (n - 2) * RELAY
@@ -488,8 +494,8 @@
                 def _(r):
                     stage(layer, r)
 
-        def relays(low, high):
-            for layer in range(layers):
+        def relays(low, high, which):
+            for layer in which:
                 for way in range(2):
                     place = places[way]
                     inner = (place >= low) & (place < high)
@@ -501,7 +507,9 @@
                 copy.wait()
 
         last = layers - 1
-        relays(1, 2)
+        if FAR_FIRST:
+            relays(2, n - 1, [last])
+        relays(1, 2, range(layers))
         chunks(lambda _, c: pass_cross(c), -TURN, 0)
         for layer in range(layers):
             for way in range(2):
@@ -513,7 +521,7 @@
         grid_rows(finish, finish_at + HOLD, last, plan=held)
         for layer in range(layers):
             grid_rows(attend, 0, layer)
-        relays(2, n - 1)
+        relays(2, n - 1, range(last) if FAR_FIRST else range(layers))
         for layer in range(layers):
             grid_rows(multiply, share_at, layer)
 
@@ -538,10 +546,8 @@
     def _(q):
         hand_partner(q)
 
-    for q in range(per):
-        for source in range(n):
-            there = out_at(q, source * width + (1 - core) * half, half)
-            remote(there, there, fp_s, fp_r.at[source, q], "tp", partner).wait_recv()
+    every = xs.at[0, :, 0:half]
+    remote(every, every, fp_s, fp_r, "tp", partner).wait_recv()
 
     def sent(ref, sem, recv):
         remote(ref, ref, sem, recv, "tp", partner).wait_send()
@@ -550,24 +556,30 @@
     sent(away, sp_s, sp_r.at[0])
     sent(away, spx_s, spx_r.at[0])
     sent(away, fin_s, fin_r.at[0, 0])
-    sent(fin, fx_s, fx_r.at[0, 0])
-    sent(xs.at[0, :, 0:half], fp_s, fp_r.at[0, 0])
-    sent(xs.at[0, 0:tokens - own, 0:half], fresh_s.at[0], fresh_r.at[0, 0])
+    sent(fin, fx_s, fx_r.at[0])
+    sent(xs.at[0, :, 0:half], fp_s, fp_r)
+    sent(xs.at[0, 0:tokens - own, 0:half], fresh_s.at[0], fresh_r.at[0])
     for layer in range(layers):
         if layer > 0:
-            sent(xs.at[layer, :, 0:half], fresh_s.at[layer], fresh_r.at[layer, 0])
-        sent(give.at[layer], gv_s.at[layer], gv_r.at[layer, 0])
+            sent(xs.at[layer, :, 0:half], fresh_s.at[layer], fresh_r.at[0])
+        sent(give.at[layer], gv_s.at[layer], gv_r.at[0])
         swapped = pair.at[layer] if layer < layers - 1 else pair.at[layer, :, 0:quarter]
         sent(swapped, cr_s.at[layer], cr_r.at[layer, 0])
         for way in range(2):
             @pl.when(places[way] < n - 1)
             def _(way=way):
-                sent(outbox.at[layer, way], ch_s.at[layer, way], ch_r.at[layer, way, 0, 0])
-                sent(box.at[layer, way], at_s.at[layer, way], at_r.at[layer, way, 0])
+                sent(outbox.at[layer, way], ch_s.at[layer, way], ch_r.at[way, 0, 0])
+                sent(box.at[layer, way], at_s.at[layer, way], at_r.at[way, 0])
 
             @pl.when(me != ends[way])
             def _(way=way):
-                sent(sq_own.at[layer], sq_s.at[layer, way], sq_r.at[layer, 0, 0])
+                sent(sq_own.at[layer], sq_s.at[layer, way], sq_r.at[0])
+
+
+def store_kernel(mixed_ref, out_ref, sem):
+    copy = pltpu.make_async_copy(mixed_ref, out_ref, sem)
+    copy.start()
+    copy.wait()
 
 
 def staged(tokens, norm_gain, w_query, w_key, w_value, w_out, offset_bias):
@@ -580,14 +592,11 @@
     count, per = total // CHUNK, own // CHUNK
     dma = pltpu.SemaphoreType.DMA
     bf16, f32 = jnp.bfloat16, jnp.float32
-    gap = jnp.zeros((*offset_bias.shape[:3], 2 * GRID_W - 2 * KC + 1), f32)
-    base = jnp.concatenate([offset_bias[..., KC - 1:], gap, offset_bias[..., :KC - 1]], axis=-1)
-    base = jnp.pad(base, ((0, 0), (0, 0), (0, 1), (0, 0)))
     space = pltpu.VMEM
     whole, anywhere = pl.BlockSpec(memory_space=space), pl.BlockSpec(memory_space=pl.ANY)
-    return pl.pallas_call(
+    mixed = pl.pallas_call(
         functools.partial(pipeline_kernel, n, m),
-        out_shape=jax.ShapeDtypeStruct((own, features), bf16),
+        out_shape=space((own, features), bf16),
         in_specs=[whole] * 3 + [anywhere] * 4,
         out_specs=whole,
         scratch_shapes=[
@@ -599,22 +608,32 @@
             space((layers, total, 3 * cols), bf16),
             space((layers, heads, 2 * KR - 2, CHUNK, 2 * GRID_W), f32),
             space((layers, count, 8, 128), f32),
-            space((layers, n, count, 8, 128), f32),
+            space((layers, count, n, 8, 128), f32),
             space((layers, 2, total, cols), bf16),
             *[space((layers, total, width // 2), bf16)] * 4,
             space((total, width // 4), bf16),
+            space((layers, 2 * heads, 2 * KR, 2 * GRID_W), f32),
             dma((layers, 4)),
-            dma, dma((count,)), dma, dma((count,)), dma((layers,)), dma((layers, count)),
-            dma((layers, 2)), dma((layers, 2, count, PARTS)), dma((layers, 2)), dma((layers, n, count)),
-            dma((layers, 2)), dma((layers, 2, count)),
-            dma((layers,)), dma((layers, count)), dma((layers,)), dma((layers, count)),
-            dma, dma((n, per)), dma, dma((n, per)), dma, dma((n, per)),
+            dma, dma((count,)), dma, dma((count,)), dma((layers,)), dma((count,)),
+            dma((layers, 2)), dma((2, count, PARTS)), dma((layers, 2)), dma((count,)),
+            dma((layers, 2)), dma((2, count)),
+            dma((layers,)), dma((count,)), dma((layers,)), dma((layers, count)),
+            dma, dma((n, per)), dma, dma((per,)), dma, dma,
         ],
         compiler_params=pltpu.CompilerParams(
             collective_id=1, has_side_effects=True, vmem_limit_bytes=VMEM_MOST
         ),
         name="pipeline",
-    )(tokens, norm_gain, base, w_query, w_key, w_value, w_out)
+    )(tokens, norm_gain, offset_bias, w_query, w_key, w_value, w_out)
+    return pl.pallas_call(
+        store_kernel,
+        out_shape=jax.ShapeDtypeStruct((own, features), bf16),
+        in_specs=[whole],
+        out_specs=anywhere,
+        scratch_shapes=[dma],
+        compiler_params=pltpu.CompilerParams(vmem_limit_bytes=2**20),
+        name="store",
+    )(mixed)
 
 
 def on_device(tokens, norm_gain, w_query, w_key, w_value, w_out, offset_bias):

time: 184 us -> 177 us (0.962)
  local copies, waits for them, and re-layouts: 5.61 us -> 1.46 us
  Pallas kernels: 177 us -> 175 us
    unnamed x3 -> x1, local copies, waits for them, and re-layouts: 3.98 us -> 1.46 us
    pallas_call x1 -> x2, Pallas kernels: 177 us -> 175 us  [the longest x1 174 us: staged(): pl.pallas_call(functools.partial(pipeline_kernel, n, m), out_shape=space(...]
where the time goes in v3:
time: 177 us
  Pallas kernels  175 us (99%)
    pallas_call x1, Pallas kernels, staged(): pl.pallas_call(functools.partial(pipeline_kernel, n, m), out_shape=space(...  174 us

profile of v3, /device:TPU:29, one launch (start us, length us, event | category | flops | bytes accessed | tf_op | source)
XLA Modules:
  0.0 176.8 jit_solution(2890037058713924564)
XLA Ops:
  0.0 1.5 copy.8.offset_ref
  1.5 174.0 %pipeline.1.mixed_ref = bf16[256,4096]{1,0:T(8,128)(2,1)S(1)} custom-call(bf16[256,4096]{1,0:T(8,128)(2,1)} %tok_ref.1, bf16[2,4096]{1,0:T(2,128)(2,1)} %gain_ref.1, f32[2,4,15,31]{3,2,1,0:T(8,128)} %copy.8.offset_ref, bf16[2,1024,512]{2,1,0:T(8,128)(2,1)} %wq_any.1, bf16[2,1024,512]{2,1,0:T(8,128)(2,1)} %wk_any.1, bf16[2,1024,512]{2,1,0:T(8,128)(2,1)} %wv_any.1, ...), custom_call_target="tpu_custom_call" | custom-call | tf_op jit(solution)/shard_map/pipeline/pallas_call | solution.py:597
  175.5 1.3 store.1

commit v4 on v3

--- a/solution.py
+++ b/solution.py
@@ -123,8 +123,11 @@
 PARTS = 3
 FIRST, RELAY = 2, 1
 MEET, CROSS, FRESH = 0, 2, 0
-HOLD = 6
-FAR_FIRST = True
+HOLD = 5
+FAR = 1
+SPREAD = 0
+HOP_TWO = 0
+LAST_RELAY = 1
 
 
 def greet(peers):
@@ -164,8 +167,8 @@
 
 
 def pipeline_kernel(
-    n, m, tok_ref, gain_ref, offset_ref, wq_any, wk_any, wv_any, wo_any, out_ref,
-    wq, wk, wv, wo, xs, part, outbox, inbox, qkv, bias, sq_own, sq_in, box,
+    n, m, tok_any, gain_ref, offset_ref, wq_any, wk_any, wv_any, wo_any, out_ref,
+    tok_ref, wq, wk, wv, wo, xs, part, outbox, inbox, qkv, bias, sq_own, sq_in, box,
     give, take, pair, cross_in, fin, padded,
     w_sem, sp_s, sp_r, spx_s, spx_r, fresh_s, fresh_r, ch_s, ch_r, sq_s, sq_r,
     at_s, at_r, gv_s, gv_r, cr_s, cr_r, fin_s, fin_r, fx_s, fx_r, fp_s, fp_r,
@@ -191,6 +194,8 @@
     places = (me, n - 1 - me)
     afters = (me + 1, me - 1)
 
+    loaded = pltpu.make_async_copy(tok_any, tok_ref, w_sem.at[0, 4])
+    loaded.start()
     weights = []
     for layer in range(layers):
         for i, (any_ref, ref) in enumerate(((wq_any, wq), (wk_any, wk), (wv_any, wv), (wo_any, wo))):
@@ -200,6 +205,7 @@
     greet(
         [("sp", lax.rem(me + k, n)) for k in range(1, n)] + [("tp", partner), ("tp", cross)]
     )
+    loaded.wait()
 
     def rows_of(c):
         return span(c * CHUNK, CHUNK)
@@ -385,8 +391,8 @@
             gv_s.at[layer], gv_r.at[r], "tp", partner,
         )
 
-    def cross_copy(layer, r):
-        at = slice(None) if layer < layers - 1 else span((1 - side) * quarter, quarter)
+    def cross_copy(layer, r, whole):
+        at = slice(None) if whole else span((1 - side) * quarter, quarter)
         rows = rows_of(r)
         return remote(
             pair.at[layer, rows, at], cross_in.at[layer, rows, at],
@@ -415,37 +421,45 @@
         pair[layer, rows, :] = (
             pair[layer, rows, :].astype(jnp.float32) + take[layer, rows, :].astype(jnp.float32)
         ).astype(jnp.bfloat16)
-        cross_copy(layer, r).start()
+        if layer < layers - 1:
+            cross_copy(layer, r, True).start()
+            return
+        owner = lax.div(r, per)
+        pl.when(owner == me)(lambda: cross_copy(layer, r, True).start())
+        pl.when(owner != me)(lambda: cross_copy(layer, r, False).start())
 
     def out_at(q, lane, size):
         return out_ref.at[span(q * CHUNK, CHUNK), span(lane, size)]
 
     def finish(layer, r):
         rows = rows_of(r)
-        cross_copy(layer, r).wait_recv()
 
         def new(at, sub):
             branch = pair[layer, rows, sub].astype(jnp.float32) + cross_in[layer, rows, sub].astype(jnp.float32)
             return (xs[layer, rows, at].astype(jnp.float32) + branch).astype(jnp.bfloat16)
 
         if layer < layers - 1:
+            cross_copy(layer, r, True).wait_recv()
             here = xs.at[layer + 1, rows, lanes]
             here[...] = new(lanes, slice(None))
             remote(here, here, fresh_s.at[layer + 1], fresh_r.at[r], "tp", partner).start()
             return
         owner, q = lax.div(r, per), lax.rem(r, per)
-        here = out_at(q, me * width + mine_q, quarter)
-        value = new(span(mine_q, quarter), span(side * quarter, quarter))
-
         @pl.when(owner == me)
         def _():
-            here[...] = value
-            remote(here, here, fx_s, fx_r.at[q], "tp", cross).start()
+            cross_copy(layer, r, True).wait_recv()
+            here = out_at(q, me * width + core * half, half)
+            here[...] = new(lanes, slice(None))
+            remote(here, here, fp_s, fp_r, "tp", partner).start()
 
         @pl.when(owner != me)
         def _():
-            fin[rows, :] = value
-            remote(fin.at[rows, :], here, fin_s, fin_r.at[me, q], "sp", owner).start()
+            cross_copy(layer, r, False).wait_recv()
+            fin[rows, :] = new(span(mine_q, quarter), span(side * quarter, quarter))
+            remote(
+                fin.at[rows, :], out_at(q, me * width + mine_q, quarter),
+                fin_s, fin_r.at[me, q], "sp", owner,
+            ).start()
 
     def hand_cross(q):
         for k in range(1, n):
@@ -455,20 +469,24 @@
             remote(here, here, fx_s, fx_r.at[q], "tp", cross).start()
 
     def hand_partner(q):
-        every = fin.at[0:n * CHUNK, :]
+        every = fin.at[0:(n - 1) * CHUNK, :]
         remote(every, every, fx_s, fx_r.at[q], "tp", cross).wait_recv()
-        for source in range(n):
+        for k in range(1, n):
+            source = lax.rem(me + k, n)
             here = out_at(q, source * width + core * half, half)
             remote(here, here, fp_s, fp_r, "tp", partner).start()
 
-    through = (n - 1) * HOP
+    through = (n - 1) * HOP - HOP_TWO
     share_at = FIRST + (n - 2) * RELAY
     meet_at = share_at + MEET
     finish_at = meet_at + CROSS
     settle = finish_at + FRESH
+    last_share = FIRST + (n - 2) * LAST_RELAY
+    last_meet = last_share + MEET
+    last_finish = last_meet + CROSS
     starts = [layer * (through + KR - 1 + settle) for layer in range(layers)]
     plans = [row_plan(count, layer == layers - 1) for layer in range(layers)]
-    final = starts[-1] + through + KR - 1 + len(plans[-1]) + finish_at
+    final = starts[-1] + through + KR - 1 + len(plans[-1]) + last_finish
 
     @pl.loop(-LEAD, final)
     def _(tick):
@@ -479,7 +497,7 @@
             def _():
                 stage(layer, c)
 
-        def grid_rows(stage, late, layer, extra=True, plan=None):
+        def grid_rows(stage, late, layer, extra=True, plan=None, behind=None):
             j = tick - late - starts[layer] - through - (KR - 1)
             plan = plan or plans[layer]
 
@@ -493,13 +511,20 @@
                 @pl.loop(first, first + size)
                 def _(r):
                     stage(layer, r)
+                    if behind:
+                        pl.when(r > first)(lambda: behind(layer, r - 1))
+
+                if behind:
+                    behind(layer, first + size - 1)
+
+        lead = per * me + OWN_LEAD if SPREAD == 0 else jnp.where(me == 1, LEAD, per * me + OWN_LEAD)
 
         def relays(low, high, which):
             for layer in which:
                 for way in range(2):
                     place = places[way]
                     inner = (place >= low) & (place < high)
-                    grid_rows(functools.partial(relay, way), FIRST + (place - 1) * RELAY, layer, inner)
+                    grid_rows(functools.partial(relay, way), FIRST + (place - 1) * (RELAY if layer < layers - 1 else LAST_RELAY), layer, inner)
 
         @pl.when(tick == 0)
         def _():
@@ -507,26 +532,36 @@
                 copy.wait()
 
         last = layers - 1
-        if FAR_FIRST:
+        if FAR == 0:
             relays(2, n - 1, [last])
         relays(1, 2, range(layers))
+        if FAR == 1:
+            relays(2, n - 1, range(layers))
         chunks(lambda _, c: pass_cross(c), -TURN, 0)
         for layer in range(layers):
             for way in range(2):
-                chunks(functools.partial(link, way), HOP * places[way], layer, places[way] > 0)
+                place = places[way]
+                early = (place > 0) & (place != 2) if HOP_TWO else place > 0
+                chunks(functools.partial(link, way), HOP * place - jnp.where(place >= 2, HOP_TWO, 0), layer, early)
         for layer in range(last):
             grid_rows(finish, finish_at, layer)
         held = plans[last][HOLD + 1:]
         held = [(0, held[0][0])] + held
-        grid_rows(finish, finish_at + HOLD, last, plan=held)
+        grid_rows(finish, last_finish + HOLD, last, plan=held)
         for layer in range(layers):
             grid_rows(attend, 0, layer)
-        relays(2, n - 1, range(last) if FAR_FIRST else range(layers))
-        for layer in range(layers):
+        if FAR != 1:
+            relays(2, n - 1, range(last) if FAR == 0 else range(layers))
+        if HOP_TWO:
+            for layer in range(layers):
+                for way in range(2):
+                    chunks(functools.partial(link, way), 2 * HOP - HOP_TWO, layer, places[way] == 2)
+        for layer in range(last):
             grid_rows(multiply, share_at, layer)
+        grid_rows(multiply, last_share, last, behind=meet)
 
         chunks(lambda _, c: pass_partner(c), -PASS, 0)
-        chunks(lambda _, c: scatter(c), -jnp.where(me == 0, OWN_LEAD, LEAD), 0)
+        chunks(lambda _, c: scatter(c), -lead, 0)
 
         @pl.when((tick >= -1) & (tick < 2 * KR - 3) & at_end)
         def _():
@@ -535,7 +570,7 @@
         for layer in range(layers):
             chunks(prepare, jnp.where(at_end, 0, HOP - 1), layer)
             chunks(first_link, 0, layer, at_end)
-        for layer in range(layers):
+        for layer in range(last):
             grid_rows(meet, meet_at, layer)
 
     @pl.loop(0, per)
@@ -556,15 +591,18 @@
     sent(away, sp_s, sp_r.at[0])
     sent(away, spx_s, spx_r.at[0])
     sent(away, fin_s, fin_r.at[0, 0])
-    sent(fin, fx_s, fx_r.at[0])
+    sent(away, fx_s, fx_r.at[0])
     sent(xs.at[0, :, 0:half], fp_s, fp_r)
     sent(xs.at[0, 0:tokens - own, 0:half], fresh_s.at[0], fresh_r.at[0])
     for layer in range(layers):
         if layer > 0:
             sent(xs.at[layer, :, 0:half], fresh_s.at[layer], fresh_r.at[0])
         sent(give.at[layer], gv_s.at[layer], gv_r.at[0])
-        swapped = pair.at[layer] if layer < layers - 1 else pair.at[layer, :, 0:quarter]
-        sent(swapped, cr_s.at[layer], cr_r.at[layer, 0])
+        if layer < layers - 1:
+            sent(pair.at[layer], cr_s.at[layer], cr_r.at[layer, 0])
+        else:
+            sent(fin, cr_s.at[layer], cr_r.at[layer, 0])
+            sent(fin.at[0:own, :], cr_s.at[layer], cr_r.at[layer, 0])
         for way in range(2):
             @pl.when(places[way] < n - 1)
             def _(way=way):
@@ -597,10 +635,10 @@
     mixed = pl.pallas_call(
         functools.partial(pipeline_kernel, n, m),
         out_shape=space((own, features), bf16),
-        in_specs=[whole] * 3 + [anywhere] * 4,
+        in_specs=[anywhere] + [whole] * 2 + [anywhere] * 4,
         out_specs=whole,
         scratch_shapes=[
-            *[space(w.shape, bf16) for w in (w_query, w_key, w_value, w_out)],
+            *[space(w.shape, bf16) for w in (tokens, w_query, w_key, w_value, w_out)],
             space((layers, total, width), bf16),
             space((2, total, 3 * cols), f32),
             space((layers, 2, total, 3 * cols), bf16),
@@ -613,7 +651,7 @@
             *[space((layers, total, width // 2), bf16)] * 4,
             space((total, width // 4), bf16),
             space((layers, 2 * heads, 2 * KR, 2 * GRID_W), f32),
-            dma((layers, 4)),
+            dma((layers, 5)),
             dma, dma((count,)), dma, dma((count,)), dma((layers,)), dma((count,)),
             dma((layers, 2)), dma((2, count, PARTS)), dma((layers, 2)), dma((count,)),
             dma((layers, 2)), dma((2, count)),

time: 177 us -> 160 us (0.904)
  Pallas kernels: 175 us -> 158 us
    pallas_call x1, Pallas kernels: 174 us -> 157 us  [staged(): pl.pallas_call(functools.partial(pipeline_kernel, n, m), out_shape=space(...]
where the time goes in v4:
time: 160 us
  Pallas kernels  158 us (99%)
    pallas_call x1, Pallas kernels, staged(): pl.pallas_call(functools.partial(pipeline_kernel, n, m), out_shape=space(...  157 us

profile of v4, /device:TPU:29, one launch (start us, length us, event | category | flops | bytes accessed | tf_op | source)
XLA Modules:
  0.0 159.6 jit_solution(8807297344156907281)
XLA Ops:
  0.0 1.5 copy.8.offset_ref
  1.5 156.8 %pipeline.1.mixed_ref = bf16[256,4096]{1,0:T(8,128)(2,1)S(1)} custom-call(bf16[256,4096]{1,0:T(8,128)(2,1)} %tok_any.1, bf16[2,4096]{1,0:T(2,128)(2,1)} %gain_ref.1, f32[2,4,15,31]{3,2,1,0:T(8,128)} %copy.8.offset_ref, bf16[2,1024,512]{2,1,0:T(8,128)(2,1)} %wq_any.1, bf16[2,1024,512]{2,1,0:T(8,128)(2,1)} %wk_any.1, bf16[2,1024,512]{2,1,0:T(8,128)(2,1)} %wv_any.1, ...), custom_call_target="tpu_custom_call" | custom-call | tf_op jit(solution)/shard_map/pipeline/pallas_call | solution.py:635
  158.3 1.3 store.1

commit v5 on v4

--- a/solution.py
+++ b/solution.py
@@ -123,11 +123,15 @@
 PARTS = 3
 FIRST, RELAY = 2, 1
 MEET, CROSS, FRESH = 0, 2, 0
-HOLD = 5
 FAR = 1
 SPREAD = 0
 HOP_TWO = 0
 LAST_RELAY = 1
+DIRECT = 0
+MORE = 0
+GROUPS = [(0, 0, 8), (2, 0, 2), (2, 2, 2), (3, 0, 4)]
+LAST_DIRECT = 0
+DIRECT_LAG = 2
 
 
 def greet(peers):
@@ -149,9 +153,16 @@
 
 
 def row_plan(count, last):
+    need = [min(max(r + KR - 1 - KR // 2, KR - 1), count - 1) - KR + 1 for r in range(count)]
+    if not last and not DIRECT:
+        return [(r, 1) for r in range(count)]
     if not last:
-        return [(r, 1) for r in range(count)]
-    need = [min(max(r + KR - 1 - KR // 2, KR - 1), count - 1) - KR + 1 for r in range(count)]
+        plan, done = [], 0
+        while done < count:
+            ready = sum(v <= len(plan) for v in need) - done
+            plan.append((done, min(ready, 2)))
+            done += plan[-1][1]
+        return plan
     ticks = need[-1]
     early = sum(v < ticks for v in need)
     sizes = [early // ticks + (t >= ticks - early % ticks) for t in range(ticks)] + [count - early]
@@ -258,6 +269,9 @@
                 part[way, rows, j * cols:(j + 1) * cols] = jnp.dot(
                     gained, w_ref[layer, :, lo:lo + cols], preferred_element_type=jnp.float32
                 )
+
+    def measure(layer, c):
+        wide = xs[layer, rows_of(c), :].astype(jnp.float32)
         squares = wide * wide
         high = squares.astype(jnp.bfloat16)
         low = (squares - high.astype(jnp.float32)).astype(jnp.bfloat16)
@@ -348,41 +362,60 @@
     way_here = jnp.where(me == 0, 0, 1)
     after_here = jnp.where(me == 0, 1, n - 2)
 
-    def attend(layer, r):
+    def direct(layer, r):
+        return r < DIRECT if layer < layers - 1 else r >= count - LAST_DIRECT
+
+    def publish(layer, r):
+        here = box.at[layer, way_here, rows_of(r), :]
+
+        def send(to):
+            remote(
+                here, here, at_s.at[layer, way_here], at_r.at[way_here, r], "sp", to
+            ).start()
+
+        @pl.when(direct(layer, r))
+        def _():
+            for k in range(n - 1, 0, -1):
+                send(jnp.where(me == 0, k, n - 1 - k))
+
+        pl.when(jnp.logical_not(direct(layer, r)))(lambda: send(after_here))
+
+    def attend(layer, r, several=1):
         @pl.when(at_end)
         def _():
-            first = jnp.clip(r - KR // 2, 0, count - KR)
-            a = first - r + KR - 1
-            rows = rows_of(r)
-            band = pl.ds(pl.multiple_of(first * CHUNK, CHUNK), KR * CHUNK)
-            outs = []
-            for h in range(heads):
-                at = [j * cols + h * HD for j in range(3)]
-                q = qkv[layer, rows, at[0]:at[0] + HD]
-                k = qkv[layer, band, at[1]:at[1] + HD]
-                v = qkv[layer, band, at[2]:at[2] + HD]
-                scores = lax.dot_general(
-                    q, k, (((1,), (1,)), ((), ())), preferred_element_type=jnp.float32
-                )
-                table = jnp.concatenate([bias[layer, h, a + 2 * i] for i in range(KR // 2)], axis=1)
-                scores = scores * scale + table
-                scores = jnp.exp(scores - jnp.max(scores, axis=-1, keepdims=True))
-                total = jnp.sum(scores, axis=-1, keepdims=True)
-                out = jnp.dot(scores.astype(jnp.bfloat16), v, preferred_element_type=jnp.float32)
-                outs.append(out / total)
-            box[layer, way_here, rows, :] = jnp.concatenate(outs, axis=1).astype(jnp.bfloat16)
-            here = box.at[layer, way_here, rows, :]
-            remote(
-                here, here, at_s.at[layer, way_here], at_r.at[way_here, r], "sp", after_here
-            ).start()
+            jobs = []
+            for i in range(several):
+                first = jnp.clip(r + i - KR // 2, 0, count - KR)
+                band = pl.ds(pl.multiple_of(first * CHUNK, CHUNK), KR * CHUNK)
+                for h in range(heads):
+                    at = [slice(j * cols + h * HD, j * cols + (h + 1) * HD) for j in range(3)]
+                    scores = lax.dot_general(
+                        qkv[layer, rows_of(r + i), at[0]], qkv[layer, band, at[1]],
+                        (((1,), (1,)), ((), ())), preferred_element_type=jnp.float32,
+                    )
+                    a = first - r - i + KR - 1
+                    table = jnp.concatenate([bias[layer, h, a + 2 * b] for b in range(KR // 2)], axis=1)
+                    jobs.append((scores * scale + table, band, at[2]))
+            jobs = [(jnp.exp(w - jnp.max(w, axis=-1, keepdims=True)), b, v) for w, b, v in jobs]
+            outs = [
+                jnp.dot(w.astype(jnp.bfloat16), qkv[layer, b, v], preferred_element_type=jnp.float32)
+                / jnp.sum(w, axis=-1, keepdims=True)
+                for w, b, v in jobs
+            ]
+            for i in range(several):
+                both = jnp.concatenate(outs[i * heads:(i + 1) * heads], axis=1)
+                box[layer, way_here, rows_of(r + i), :] = both.astype(jnp.bfloat16)
+                publish(layer, r + i)
 
     def box_copy(layer, way, r):
         here = box.at[layer, way, rows_of(r), :]
         return remote(here, here, at_s.at[layer, way], at_r.at[way, r], "sp", afters[way])
 
     def relay(way, layer, r):
-        box_copy(layer, way, r).wait_recv()
-        box_copy(layer, way, r).start()
+        @pl.when(jnp.logical_not(direct(layer, r)))
+        def _():
+            box_copy(layer, way, r).wait_recv()
+            box_copy(layer, way, r).start()
 
     def give_copy(layer, r):
         rows = rows_of(r)
@@ -401,7 +434,7 @@
 
     def multiply(layer, r):
         for way in range(2):
-            @pl.when(places[way] == n - 1)
+            @pl.when((places[way] == n - 1) | ((places[way] > 0) & direct(layer, r)))
             def _(way=way):
                 box_copy(layer, way, r).wait_recv()
         rows = rows_of(r)
@@ -477,16 +510,23 @@
             remote(here, here, fp_s, fp_r, "tp", partner).start()
 
     through = (n - 1) * HOP - HOP_TWO
-    share_at = FIRST + (n - 2) * RELAY
+    plans = [row_plan(count, layer == layers - 1) for layer in range(layers)]
+    share_at = 0
+    for j, (first, size) in enumerate(plans[0]):
+        for row in range(first, first + size):
+            late = DIRECT_LAG if row < DIRECT else FIRST + (n - 2) * RELAY
+            share_at = max(share_at, j + late - row)
     meet_at = share_at + MEET
     finish_at = meet_at + CROSS
     settle = finish_at + FRESH
-    last_share = FIRST + (n - 2) * LAST_RELAY
-    last_meet = last_share + MEET
-    last_finish = last_meet + CROSS
+    last_share = FIRST + (n - 2) * LAST_RELAY + MORE
+    last_finish = last_share + MEET + CROSS
     starts = [layer * (through + KR - 1 + settle) for layer in range(layers)]
-    plans = [row_plan(count, layer == layers - 1) for layer in range(layers)]
-    final = starts[-1] + through + KR - 1 + len(plans[-1]) + last_finish
+    singles = [(row, 1) for row in range(count)]
+    shares = plans[-1]
+    if LAST_DIRECT:
+        shares = shares[:-2] + [(shares[-2][0], shares[-2][1] + shares[-1][1])]
+    final = starts[-1] + through + KR - 1 + len(shares) + last_finish
 
     @pl.loop(-LEAD, final)
     def _(tick):
@@ -544,10 +584,10 @@
                 early = (place > 0) & (place != 2) if HOP_TWO else place > 0
                 chunks(functools.partial(link, way), HOP * place - jnp.where(place >= 2, HOP_TWO, 0), layer, early)
         for layer in range(last):
-            grid_rows(finish, finish_at, layer)
-        held = plans[last][HOLD + 1:]
-        held = [(0, held[0][0])] + held
-        grid_rows(finish, last_finish + HOLD, last, plan=held)
+            grid_rows(finish, finish_at, layer, plan=singles)
+        groups = [(i * per + a, b) for i, a, b in GROUPS]
+        waits = len(shares) - len(groups)
+        grid_rows(finish, last_finish + waits, last, plan=groups)
         for layer in range(layers):
             grid_rows(attend, 0, layer)
         if FAR != 1:
@@ -557,25 +597,23 @@
                 for way in range(2):
                     chunks(functools.partial(link, way), 2 * HOP - HOP_TWO, layer, places[way] == 2)
         for layer in range(last):
-            grid_rows(multiply, share_at, layer)
-        grid_rows(multiply, last_share, last, behind=meet)
-
-        chunks(lambda _, c: pass_partner(c), -PASS, 0)
-        chunks(lambda _, c: scatter(c), -lead, 0)
-
-        @pl.when((tick >= -1) & (tick < 2 * KR - 3) & at_end)
-        def _():
-            make_bias(tick + 1)
-
+            grid_rows(multiply, share_at, layer, plan=singles)
+        grid_rows(multiply, last_share, last, plan=shares, behind=meet)
         for layer in range(layers):
             chunks(prepare, jnp.where(at_end, 0, HOP - 1), layer)
             chunks(first_link, 0, layer, at_end)
         for layer in range(last):
-            grid_rows(meet, meet_at, layer)
-
-    @pl.loop(0, per)
-    def _(q):
-        hand_cross(q)
+            grid_rows(meet, meet_at, layer, plan=singles)
+        for layer in range(layers):
+            chunks(measure, jnp.where(at_end, 0, HOP - 1), layer)
+        chunks(lambda _, c: pass_partner(c), -PASS, 0)
+        chunks(lambda _, c: scatter(c), -lead, 0)
+
+        @pl.when((tick >= -1) & (tick < 2 * KR - 3) & at_end)
+        def _():
+            make_bias(tick + 1)
+
+    pl.loop(0, per)(hand_cross)
 
     @pl.loop(0, per)
     def _(q):
@@ -607,7 +645,13 @@
             @pl.when(places[way] < n - 1)
             def _(way=way):
                 sent(outbox.at[layer, way], ch_s.at[layer, way], ch_r.at[way, 0, 0])
-                sent(box.at[layer, way], at_s.at[layer, way], at_r.at[way, 0])
+                straight = DIRECT if layer < layers - 1 else LAST_DIRECT
+                sent(box.at[layer, way, straight * CHUNK:, :], at_s.at[layer, way], at_r.at[way, 0])
+                if straight:
+                    @pl.when(places[way] == 0)
+                    def _():
+                        several = box.at[layer, way, 0:(n - 1) * straight * CHUNK, :]
+                        sent(several, at_s.at[layer, way], at_r.at[way, 0])
 
             @pl.when(me != ends[way])
             def _(way=way):

time: 160 us -> 157 us (0.981)
  Pallas kernels: 158 us -> 155 us
    pallas_call x1, Pallas kernels: 157 us -> 154 us  [staged(): pl.pallas_call(functools.partial(pipeline_kernel, n, m), out_shape=space(...]
where the time goes in v5:
time: 157 us; the launch traced here: 156 us
  Pallas kernels  155 us (99%)
    pallas_call x1, Pallas kernels, staged(): pl.pallas_call(functools.partial(pipeline_kernel, n, m), out_shape=space(...  154 us

profile of v5, /device:TPU:29, one launch (start us, length us, event | category | flops | bytes accessed | tf_op | source)
XLA Modules:
  0.0 156.4 jit_solution(11564277674837688069)
XLA Ops:
  0.0 1.5 copy.8.offset_ref
  1.5 153.6 %pipeline.1.mixed_ref = bf16[256,4096]{1,0:T(8,128)(2,1)S(1)} custom-call(bf16[256,4096]{1,0:T(8,128)(2,1)} %tok_any.1, bf16[2,4096]{1,0:T(2,128)(2,1)} %gain_ref.1, f32[2,4,15,31]{3,2,1,0:T(8,128)} %copy.8.offset_ref, bf16[2,1024,512]{2,1,0:T(8,128)(2,1)} %wq_any.1, bf16[2,1024,512]{2,1,0:T(8,128)(2,1)} %wk_any.1, bf16[2,1024,512]{2,1,0:T(8,128)(2,1)} %wv_any.1, ...), custom_call_target="tpu_custom_call" | custom-call | tf_op jit(solution)/shard_map/pipeline/pallas_call | solution.py:679
  155.1 1.3 store.1

commit v6 on v5

--- a/solution.py
+++ b/solution.py
@@ -280,7 +280,7 @@
         total = lax.dot_general(
             ones, high, nt, preferred_element_type=jnp.float32
         ) + lax.dot_general(ones, low, nt, preferred_element_type=jnp.float32)
-        sq_own[layer, c] = jnp.concatenate([total] * (128 // CHUNK), axis=1)
+        sq_own[layer, c] = jnp.concatenate([total[:1]] * (128 // CHUNK), axis=1)
         for e, end in enumerate(ends):
             @pl.when(me != end)
             def _(e=e, end=end):
@@ -328,7 +328,7 @@
             for k in range(1, n):
                 squares = squares + sq_in[layer, c, lax.rem(me + k, n)]
             scaled = lax.rsqrt(squares / features + norm_eps)
-            inverse = jnp.concatenate([scaled] * 16, axis=0).T[:CHUNK, :1]
+            inverse = jnp.broadcast_to(scaled, (128, 128)).T[:CHUNK, :1]
             for i, at in enumerate(pieces):
                 qkv[layer, rows, at] = (total(i) * inverse).astype(jnp.bfloat16)
 
@@ -578,16 +578,16 @@
         if FAR == 1:
             relays(2, n - 1, range(layers))
         chunks(lambda _, c: pass_cross(c), -TURN, 0)
+        for layer in range(last):
+            grid_rows(finish, finish_at, layer, plan=singles)
+        groups = [(i * per + a, b) for i, a, b in GROUPS]
+        waits = len(shares) - len(groups)
+        grid_rows(finish, last_finish + waits, last, plan=groups)
         for layer in range(layers):
             for way in range(2):
                 place = places[way]
                 early = (place > 0) & (place != 2) if HOP_TWO else place > 0
                 chunks(functools.partial(link, way), HOP * place - jnp.where(place >= 2, HOP_TWO, 0), layer, early)
-        for layer in range(last):
-            grid_rows(finish, finish_at, layer, plan=singles)
-        groups = [(i * per + a, b) for i, a, b in GROUPS]
-        waits = len(shares) - len(groups)
-        grid_rows(finish, last_finish + waits, last, plan=groups)
         for layer in range(layers):
             grid_rows(attend, 0, layer)
         if FAR != 1:
@@ -689,8 +689,8 @@
             space((layers, 2, total, 3 * cols), bf16),
             space((layers, total, 3 * cols), bf16),
             space((layers, heads, 2 * KR - 2, CHUNK, 2 * GRID_W), f32),
-            space((layers, count, 8, 128), f32),
-            space((layers, count, n, 8, 128), f32),
+            space((layers, count, 1, 128), f32),
+            space((layers, count, n, 1, 128), f32),
             space((layers, 2, total, cols), bf16),
             *[space((layers, total, width // 2), bf16)] * 4,
             space((total, width // 4), bf16),

time: 157 us -> 153 us (0.975)
  Pallas kernels: 155 us -> 151 us
    pallas_call x1, Pallas kernels: 154 us -> 150 us  [staged(): pl.pallas_call(functools.partial(pipeline_kernel, n, m), out_shape=space(...]
where the time goes in v6:
time: 153 us
  Pallas kernels  151 us (99%)
    pallas_call x1, Pallas kernels, staged(): pl.pallas_call(functools.partial(pipeline_kernel, n, m), out_shape=space(...  150 us

profile of v6, /device:TPU:29, one launch (start us, length us, event | category | flops | bytes accessed | tf_op | source)
XLA Modules:
  0.0 152.9 jit_solution(16957173613586917016)
XLA Ops:
  0.0 1.5 copy.8.offset_ref
  1.5 150.1 %pipeline.1.mixed_ref = bf16[256,4096]{1,0:T(8,128)(2,1)S(1)} custom-call(bf16[256,4096]{1,0:T(8,128)(2,1)} %tok_any.1, bf16[2,4096]{1,0:T(2,128)(2,1)} %gain_ref.1, f32[2,4,15,31]{3,2,1,0:T(8,128)} %copy.8.offset_ref, bf16[2,1024,512]{2,1,0:T(8,128)(2,1)} %wq_any.1, bf16[2,1024,512]{2,1,0:T(8,128)(2,1)} %wk_any.1, bf16[2,1024,512]{2,1,0:T(8,128)(2,1)} %wv_any.1, ...), custom_call_target="tpu_custom_call" | custom-call | tf_op jit(solution)/shard_map/pipeline/pallas_call | solution.py:679
  151.6 1.3 store.1

commit v7 on v6

--- a/solution.py
+++ b/solution.py
@@ -604,14 +604,15 @@
             chunks(first_link, 0, layer, at_end)
         for layer in range(last):
             grid_rows(meet, meet_at, layer, plan=singles)
+        chunks(lambda _, c: pass_partner(c), -PASS, 0)
+        chunks(lambda _, c: scatter(c), -lead, 0)
+
+        @pl.when((tick >= -1) & (tick < 2 * KR - 3) & at_end)
+        def _():
+            make_bias(tick + 1)
+
         for layer in range(layers):
             chunks(measure, jnp.where(at_end, 0, HOP - 1), layer)
-        chunks(lambda _, c: pass_partner(c), -PASS, 0)
-        chunks(lambda _, c: scatter(c), -lead, 0)
-
-        @pl.when((tick >= -1) & (tick < 2 * KR - 3) & at_end)
-        def _():
-            make_bias(tick + 1)
 
     pl.loop(0, per)(hand_cross)
 

time: 153 us -> 152 us (level)
  no operation moved by 1% of the time
where the time goes in v7:
time: 152 us
  Pallas kernels  150 us (99%)
    pallas_call x1, Pallas kernels, staged(): pl.pallas_call(functools.partial(pipeline_kernel, n, m), out_shape=space(...  149 us

profile of v7, /device:TPU:29, one launch (start us, length us, event | category | flops | bytes accessed | tf_op | source)
XLA Modules:
  0.0 151.9 jit_solution(489824232057058348)
XLA Ops:
  0.0 1.5 copy.8.offset_ref
  1.5 149.1 %pipeline.1.mixed_ref = bf16[256,4096]{1,0:T(8,128)(2,1)S(1)} custom-call(bf16[256,4096]{1,0:T(8,128)(2,1)} %tok_any.1, bf16[2,4096]{1,0:T(2,128)(2,1)} %gain_ref.1, f32[2,4,15,31]{3,2,1,0:T(8,128)} %copy.8.offset_ref, bf16[2,1024,512]{2,1,0:T(8,128)(2,1)} %wq_any.1, bf16[2,1024,512]{2,1,0:T(8,128)(2,1)} %wk_any.1, bf16[2,1024,512]{2,1,0:T(8,128)(2,1)} %wv_any.1, ...), custom_call_target="tpu_custom_call" | custom-call | tf_op jit(solution)/shard_map/pipeline/pallas_call | solution.py:680
  150.5 1.3 store.1
